TPU v7x, 256 devices: a whole 4x4x8 slice. The times are simulated.
256 devices in a mesh: sp: 32 (over z, y), tp: 8 (over x, core).
Axes of the slice: x: 4, y: 4, z: 8, core: 2. Of those that a mesh axis runs over, the one named last changes fastest.
Arguments:
- resid_stream: bfloat16 [12288, 2048], P('sp'), may hold values from -6 to 6
- q_latent: bfloat16 [12288, 512], P('sp'), may hold values from -6 to 6
- kv_latent: bfloat16 [12288, 256], P('sp'), may hold values from -6 to 6
- rope_key: bfloat16 [12288, 64], P('sp'), may hold values from -6 to 6
- doc_ids: int32 [12288], P('sp'), may hold values from 0 to 3, as said below
- q_gain: float32 [512], replicated, may hold values from 1.5 to 64
- kv_gain: float32 [256], replicated, may hold values from 0.1 to 1.9
- w_query: bfloat16 [512, 3072], P(None, 'tp'), may hold values from -0.25 to 0.25
- w_key: bfloat16 [256, 2048], P(None, 'tp'), may hold values from -0.375 to 0.375
- w_value: bfloat16 [256, 2048], P(None, 'tp'), may hold values from -0.375 to 0.375
- w_out: bfloat16 [2048, 2048], replicated, may hold values from -0.5 to 0.5
- mix_gain: float32 [2048], replicated, may hold values from 0.1 to 1.9
- w_gate: bfloat16 [2048, 5632], P('sp', 'tp'), may hold values from -0.125 to 0.125
- w_up: bfloat16 [2048, 5632], P('sp', 'tp'), may hold values from -0.125 to 0.125
- w_down: bfloat16 [5632, 2048], P('tp', 'sp'), may hold values from -0.3125 to 0.3125
- out_gain: float32 [2048], replicated, may hold values from 0.1 to 1.9
Outputs:
- layer_out: bfloat16 [12288, 2048], P(('sp', 'tp'))
Inputs may be any that keep to these rules, and one draw needn't show every extreme that they name: `doc_ids`: document numbers never fall along the sequence; every document has 1 to 9216 positions and one has exactly 9216.
All inputs are finite; a program needn't handle non-finite values.
Results may differ from a plain program's by a relative error of at most 0.02.
The roundings to bfloat16 on the way count: a program that leaves them out, or rounds other values in their place, can miss the bound.
Values may be sent and summed in bfloat16 or wider, within the bound.
A program may use at most 128 MiB of HBM per device.

v0:
```python
import jax
import jax.numpy as jnp
from jax import lax
from jax.sharding import Mesh
from jax.sharding import PartitionSpec as P

NOPE = 128
RD = 64
VD = 128
SP = ("sp_0", "sp_1")
SP_TP = ("sp_0", "sp_1", "tp")


eps_norm = 1e-05
rope_theta = 10000.0
resid_alpha = 8.0**0.25
key_span = 2048


def sent_together(arrays, axis, dim, along):
    widths = [a.shape[along] for a in arrays]
    both = jnp.concatenate(arrays, axis=along)
    whole = lax.all_gather(both, axis, axis=dim, tiled=True)
    return tuple(jnp.split(whole, [sum(widths[:k]) for k in range(1, len(widths))], axis=along))


def laid_out(tiles, dim):
    tiles = jnp.moveaxis(tiles, 0, dim)
    lengths = tiles.shape
    return tiles.reshape(*lengths[:dim], lengths[dim] * lengths[dim + 1], *lengths[dim + 2 :])


def copy_for_each(value, axis):
    copies = jnp.broadcast_to(value, (lax.axis_size(axis), *value.shape))
    return lax.all_to_all(copies, axis, split_axis=0, concat_axis=0, tiled=True)


def gathered_copies(value, axis, dim):
    return laid_out(copy_for_each(value, axis), dim)


def gather_axes(value, axes, dim):
    whole = value
    for number in range(len(axes) - 1, -1, -1):
        whole = lax.all_gather(whole, axes[number], axis=dim, tiled=True)
    return whole


def in_blocks(value, dim, count):
    lengths = value.shape
    tiles = value.reshape(*lengths[:dim], count, lengths[dim] // count, *lengths[dim + 1 :])
    return jnp.moveaxis(tiles, dim, 0)


def sent_and_summed(value, axis, dim):
    count = lax.axis_size(axis)
    tiles = lax.all_to_all(in_blocks(value, dim, count), axis, 0, 0, tiled=True)
    return jnp.sum(tiles.astype(jnp.float32), axis=0)


def rope_angles(positions):
    frequency = rope_theta ** (-jnp.arange(0, RD, 2, dtype=jnp.float32) / RD)
    angles = positions.astype(jnp.float32)[:, None] * frequency[None, :]
    return (jnp.cos(angles), jnp.sin(angles))


def rotate(values, cos_table, sin_table):
    half_width = values.shape[-1] // 2
    first_half = values[..., :half_width]
    second_half = values[..., half_width:]
    return jnp.concatenate(
        [
            first_half * cos_table - second_half * sin_table,
            second_half * cos_table + first_half * sin_table,
        ],
        axis=-1,
    )


def rms_scaled(latent, scaling):
    widened = latent.astype(jnp.float32)
    inverse = lax.rsqrt(jnp.mean(widened * widened, axis=-1, keepdims=True) + eps_norm)
    return (widened * inverse * scaling).astype(jnp.bfloat16)


def layer_scaled(stream, scaling):
    centre = stream - jnp.mean(stream, axis=-1, keepdims=True)
    spread = jnp.mean(centre * centre, axis=-1, keepdims=True)
    return centre * lax.rsqrt(spread + eps_norm) * scaling


def fold_in_blocks(carried, piece_part, attend_fn):
    piece_rows = piece_part[0].shape[0]

    def one_block(inner, block_index):
        sliced = tuple(
            (
                lax.dynamic_slice_in_dim(member, block_index * key_span, key_span, 0)
                for member in piece_part
            )
        )
        return (attend_fn(inner, sliced), None)

    outcome = lax.scan(one_block, carried, jnp.arange(piece_rows // key_span, dtype=jnp.int32))
    return outcome[0]


def body(
    resid_stream,
    q_latent,
    kv_latent,
    rope_key,
    doc_ids,
    q_gain,
    kv_gain,
    w_query,
    w_key,
    w_value,
    w_out,
    mix_gain,
    w_gate,
    w_up,
    w_down,
    out_gain,
):
    tok_rows = q_latent.shape[0]
    head_count = w_key.shape[1] // NOPE
    tp_count = lax.axis_size("tp")
    part_rows = tok_rows // tp_count
    tp_index = lax.axis_index("tp")
    positions = lax.axis_index(SP) * tok_rows + jnp.arange(tok_rows, dtype=jnp.int32)
    cos_table, sin_table = rope_angles(positions)
    q_normed = rms_scaled(q_latent, q_gain)
    queries = jnp.dot(q_normed, w_query, preferred_element_type=jnp.float32).reshape(
        tok_rows, head_count, NOPE + RD
    )
    query_nope = queries[:, :, :NOPE].astype(jnp.bfloat16)
    query_rope = rotate(queries[:, :, NOPE:], cos_table[:, None, :], sin_table[:, None, :]).astype(
        jnp.bfloat16
    )
    kv_normed = rms_scaled(kv_latent, kv_gain)
    key_rot = rotate(rope_key.astype(jnp.float32), cos_table, sin_table).astype(jnp.bfloat16)
    score_scale = (NOPE + RD) ** (-0.5)

    def attend_rows(carried, piece_part):
        row_top, denom_sum, accum_out = carried
        key_piece, value_piece, rot_piece, doc_piece = piece_part
        piece_rows = key_piece.shape[0]
        keys_heads = key_piece.reshape(piece_rows, head_count, NOPE)
        values_heads = value_piece.reshape(piece_rows, head_count, VD)
        scores = jnp.einsum(
            "qhd,khd->hqk", query_nope, keys_heads, preferred_element_type=jnp.float32
        )
        scores = (
            scores
            + jnp.einsum("qhd,kd->hqk", query_rope, rot_piece, preferred_element_type=jnp.float32)
        ) * score_scale
        same_doc = (doc_ids[:, None] == doc_piece[None, :])[None]
        masked = jnp.where(same_doc, scores, -1e30)
        new_top = jnp.maximum(row_top, jnp.max(masked, axis=-1))
        weights = jnp.where(same_doc, jnp.exp(masked - new_top[:, :, None]), 0.0)
        factor = jnp.exp(row_top - new_top)
        denom_sum = denom_sum * factor + jnp.sum(weights, axis=-1)
        update = jnp.einsum(
            "hqk,khd->qhd",
            weights.astype(jnp.bfloat16),
            values_heads,
            preferred_element_type=jnp.float32,
        )
        accum_out = accum_out * jnp.transpose(factor)[:, :, None] + update
        return (new_top, denom_sum, accum_out)

    initial = (
        jnp.full((head_count, tok_rows), -1e30, jnp.float32),
        jnp.zeros((head_count, tok_rows), jnp.float32),
        jnp.zeros((tok_rows, head_count, VD), jnp.float32),
    )

    def project_rows(carried, piece_part):
        latent_piece, rot_piece, doc_piece = piece_part
        key_piece = jnp.dot(latent_piece, w_key, preferred_element_type=jnp.float32).astype(
            jnp.bfloat16
        )
        value_piece = jnp.dot(latent_piece, w_value, preferred_element_type=jnp.float32).astype(
            jnp.bfloat16
        )
        return attend_rows(carried, (key_piece, value_piece, rot_piece, doc_piece))

    carried_out = fold_in_blocks(
        initial,
        (
            *sent_together((kv_normed, key_rot), SP, 0, 1),
            lax.all_gather(doc_ids, SP, axis=0, tiled=True),
        ),
        project_rows,
    )
    denom_sum = carried_out[1]
    attended = (
        (carried_out[2] / jnp.transpose(denom_sum)[:, :, None])
        .astype(jnp.bfloat16)
        .reshape(tok_rows, head_count * VD)
    )
    heads_rows = lax.all_to_all(attended, "tp", split_axis=0, concat_axis=1, tiled=True)
    mixer_out = jnp.dot(heads_rows, w_out, preferred_element_type=jnp.float32)
    own_resid = lax.dynamic_slice_in_dim(resid_stream, tp_index * part_rows, part_rows, 0)
    own_normed = layer_scaled(
        resid_alpha * own_resid.astype(jnp.float32) + mixer_out, mix_gain
    ).astype(jnp.bfloat16)
    normed_rows = gathered_copies(own_normed, "tp", 0)
    gate_part = jnp.dot(normed_rows, gather_axes(w_gate, SP, 0), preferred_element_type=jnp.float32)
    up_part = jnp.dot(normed_rows, gather_axes(w_up, SP, 0), preferred_element_type=jnp.float32)
    hidden = (jax.nn.silu(gate_part) * up_part).astype(jnp.bfloat16)
    down_term = jnp.dot(hidden, gather_axes(w_down, SP, 1), preferred_element_type=jnp.float32)
    ffn_sum = sent_and_summed(down_term.astype(jnp.bfloat16), "tp", 0)
    layer_out = layer_scaled(
        resid_alpha * own_normed.astype(jnp.float32) + 0.5 * ffn_sum, out_gain
    ).astype(jnp.bfloat16)
    return layer_out


def solution(mesh):
    split = Mesh(mesh.devices.reshape(8, 4, mesh.shape["tp"]), ("sp_0", "sp_1", "tp"))
    in_specs = (
        P(SP, None),
        P(SP, None),
        P(SP, None),
        P(SP, None),
        P(SP),
        P(),
        P(),
        P(None, "tp"),
        P(None, "tp"),
        P(None, "tp"),
        P(),
        P(),
        P(SP, "tp"),
        P(SP, "tp"),
        P("tp", SP),
        P(),
    )
    out_specs = P(SP_TP, None)
    return jax.shard_map(body, mesh=split, in_specs=in_specs, out_specs=out_specs, check_vma=False)
```

profile of v0, /device:TPU:1, one launch (start us, length us, event | category | flops | bytes accessed | tf_op | source)
XLA Modules:
  0.0 317.2 jit_solution(13309439530731203723)
XLA Ops:
  10.5 13.0 %all_gather.26 = bf16[256,704]{1,0:T(8,128)(2,1)} all-gather(bf16[64,704]{1,0:T(8,128)(2,1)} %param.30), channel_id=1, replica_groups=mesh['sp_0'=8,'sp_1'=4,'tp'=8] {'sp_1'}, dimensions={0}, use_global_device_ids=true | all-gather | bytes 450560 | tf_op jit(solution)/shard_map/all_gather | solution.py:45
  23.6 11.2 %all_gather.28 = bf16[256,704]{1,0:T(8,128)(2,1)} all-gather(bf16[64,704]{1,0:T(8,128)(2,1)} %param.31), channel_id=1, replica_groups=mesh['sp_0'=8,'sp_1'=4,'tp'=8] {'sp_1'}, dimensions={0}, use_global_device_ids=true | all-gather | bytes 450560 | tf_op jit(solution)/shard_map/all_gather | solution.py:45
  34.9 11.2 %all_gather.30 = bf16[704,256]{0,1:T(8,128)(2,1)} all-gather(bf16[704,64]{0,1:T(8,128)(2,1)S(1)} %copy-done.5), channel_id=1, replica_groups=mesh['sp_0'=8,'sp_1'=4,'tp'=8] {'sp_1'}, dimensions={1}, use_global_device_ids=true | all-gather | bytes 450560 | tf_op jit(solution)/shard_map/all_gather | solution.py:45
  47.1 42.1 %all-gather = s32[32,1,384]{2,1,0:T(1,128)S(1)} all-gather(s32[1,1,384]{2,1,0:T(1,128)S(1)} %reshape.158), channel_id=1, replica_groups=mesh['sp_0'=8,'sp_1'=4,'tp'=8] {'sp_0','sp_1'}, dimensions={0}, use_global_device_ids=true | all-gather | bytes 50688 | tf_op jit(solution)/shard_map/all_gather | solution.py:193
  89.3 21.7 %all-gather.6.cloned.1.call-done = bf16[12288,320]{0,1:T(8,128)(2,1)} async-done(((bf16[384,320]{0,1:T(8,128)(2,1)}), bf16[12288,320]{0,1:T(8,128)(2,1)}) %all-gather.6.cloned.1.call-update) | async-done | bytes 7864336 | tf_op jit(solution)/shard_map/all_gather | solution.py:23
  110.9 6.1 %split.8 = bf16[12288,256]{0,1:T(8,128)(2,1)} slice(bf16[12288,320]{0,1:T(8,128)(2,1)} %all-gather.6.cloned.1.call-done), slice={[0:12288], [0:256]} | slice | bytes 12582912 | tf_op jit(solution)/shard_map/split | solution.py:24
  118.5 106.6 %while.15 = (s32[]{:T(128)}, f32[2,384]{1,0:T(2,128)S(1)}, f32[2,384]{1,0:T(2,128)S(1)}, f32[384,2,128]{0,2,1:T(8,128)}, s32[384]{0:T(512)S(1)}, /*index=5*/s32[...) while((s32[]{:T(128)}, f32[2,384]{1,0:T(2,128)S(1)}, ...), condition=%wide.region_5.6_spmd.clone, body=%wide.region_2.5_spmd.clone.sunk | while | flops 1561367040 | bytes 61450016 | solution.py:104
  123.1 4.6 %fusion.86 = (f32[2,384]{1,0:T(2,128)S(1)}, f32[2,384,2048]{1,2,0:T(8,128)}) fusion(f32[2048,384,2]{1,0,2:T(8,128)S(1)} %fusion.85, bf16[2048,2,128]{0,2,1:T(8,128)(2,1)S(1)} %bitcast.68, bf16[384,2,128]{2,0,1:T(8,128)(2,1)S(1)} %get-tuple-element.326, pred[384,2048]{0,1:T(8,128)(4,1)S(1)} %broadcast_compare_fusion.2), kind=kOutput, calls=%fused_computation.75.clone.1 | convolution fusion | flops 408943872 | bytes 14617600 | tf_op jit(solution)/shard_map/while/body/eval_jaxpr/qhd,khd->hqk/dot_general | solution.py:151
  127.7 1.9 convolution_convert_fusion.6
  129.6 5.3 %fusion.90 = f32[384,2,128]{0,2,1:T(8,128)} fusion(bf16[2048,2,128]{0,2,1:T(8,128)(2,1)S(1)} %bitcast.69, f32[2,384,2048]{1,2,0:T(8,128)} %get-tuple-element.281, f32[2,384]{1,0:T(2,128)S(1)} %get-tuple-element.318, pred[384,2048]{0,1:T(8,128)(4,1)S(1)} %broadcast_compare_fusion.2, f32[384,2,128]{0,2,1:T(8,128)} %get-tuple-element.303, ...), kind=kOutput, calls=%fused_computation.14.clone.1 | convolution fusion | flops 407666688 | bytes 8919041 | tf_op jit(solution)/shard_map/while/body/eval_jaxpr/hqk,khd->qhd/dot_general | solution.py:164
  140.8 4.6 %fusion.86 = (f32[2,384]{1,0:T(2,128)S(1)}, f32[2,384,2048]{1,2,0:T(8,128)}) fusion(f32[2048,384,2]{1,0,2:T(8,128)S(1)} %fusion.85, bf16[2048,2,128]{0,2,1:T(8,128)(2,1)S(1)} %bitcast.68, bf16[384,2,128]{2,0,1:T(8,128)(2,1)S(1)} %get-tuple-element.326, pred[384,2048]{0,1:T(8,128)(4,1)S(1)} %broadcast_compare_fusion.2), kind=kOutput, calls=%fused_computation.75.clone.1 | convolution fusion | flops 408943872 | bytes 14617600 | tf_op jit(solution)/shard_map/while/body/eval_jaxpr/qhd,khd->hqk/dot_general | solution.py:151
  145.4 1.9 convolution_convert_fusion.6
  147.3 5.4 %fusion.90 = f32[384,2,128]{0,2,1:T(8,128)} fusion(bf16[2048,2,128]{0,2,1:T(8,128)(2,1)S(1)} %bitcast.69, f32[2,384,2048]{1,2,0:T(8,128)} %get-tuple-element.281, f32[2,384]{1,0:T(2,128)S(1)} %get-tuple-element.318, pred[384,2048]{0,1:T(8,128)(4,1)S(1)} %broadcast_compare_fusion.2, f32[384,2,128]{0,2,1:T(8,128)} %get-tuple-element.303, ...), kind=kOutput, calls=%fused_computation.14.clone.1 | convolution fusion | flops 407666688 | bytes 8919041 | tf_op jit(solution)/shard_map/while/body/eval_jaxpr/hqk,khd->qhd/dot_general | solution.py:164
  158.6 4.6 %fusion.86 = (f32[2,384]{1,0:T(2,128)S(1)}, f32[2,384,2048]{1,2,0:T(8,128)}) fusion(f32[2048,384,2]{1,0,2:T(8,128)S(1)} %fusion.85, bf16[2048,2,128]{0,2,1:T(8,128)(2,1)S(1)} %bitcast.68, bf16[384,2,128]{2,0,1:T(8,128)(2,1)S(1)} %get-tuple-element.326, pred[384,2048]{0,1:T(8,128)(4,1)S(1)} %broadcast_compare_fusion.2), kind=kOutput, calls=%fused_computation.75.clone.1 | convolution fusion | flops 408943872 | bytes 14617600 | tf_op jit(solution)/shard_map/while/body/eval_jaxpr/qhd,khd->hqk/dot_general | solution.py:151
  163.2 1.9 convolution_convert_fusion.6
  165.1 5.3 %fusion.90 = f32[384,2,128]{0,2,1:T(8,128)} fusion(bf16[2048,2,128]{0,2,1:T(8,128)(2,1)S(1)} %bitcast.69, f32[2,384,2048]{1,2,0:T(8,128)} %get-tuple-element.281, f32[2,384]{1,0:T(2,128)S(1)} %get-tuple-element.318, pred[384,2048]{0,1:T(8,128)(4,1)S(1)} %broadcast_compare_fusion.2, f32[384,2,128]{0,2,1:T(8,128)} %get-tuple-element.303, ...), kind=kOutput, calls=%fused_computation.14.clone.1 | convolution fusion | flops 407666688 | bytes 8919041 | tf_op jit(solution)/shard_map/while/body/eval_jaxpr/hqk,khd->qhd/dot_general | solution.py:164
  176.4 4.6 %fusion.86 = (f32[2,384]{1,0:T(2,128)S(1)}, f32[2,384,2048]{1,2,0:T(8,128)}) fusion(f32[2048,384,2]{1,0,2:T(8,128)S(1)} %fusion.85, bf16[2048,2,128]{0,2,1:T(8,128)(2,1)S(1)} %bitcast.68, bf16[384,2,128]{2,0,1:T(8,128)(2,1)S(1)} %get-tuple-element.326, pred[384,2048]{0,1:T(8,128)(4,1)S(1)} %broadcast_compare_fusion.2), kind=kOutput, calls=%fused_computation.75.clone.1 | convolution fusion | flops 408943872 | bytes 14617600 | tf_op jit(solution)/shard_map/while/body/eval_jaxpr/qhd,khd->hqk/dot_general | solution.py:151
  181.0 1.9 convolution_convert_fusion.6
  182.9 5.4 %fusion.90 = f32[384,2,128]{0,2,1:T(8,128)} fusion(bf16[2048,2,128]{0,2,1:T(8,128)(2,1)S(1)} %bitcast.69, f32[2,384,2048]{1,2,0:T(8,128)} %get-tuple-element.281, f32[2,384]{1,0:T(2,128)S(1)} %get-tuple-element.318, pred[384,2048]{0,1:T(8,128)(4,1)S(1)} %broadcast_compare_fusion.2, f32[384,2,128]{0,2,1:T(8,128)} %get-tuple-element.303, ...), kind=kOutput, calls=%fused_computation.14.clone.1 | convolution fusion | flops 407666688 | bytes 8919041 | tf_op jit(solution)/shard_map/while/body/eval_jaxpr/hqk,khd->qhd/dot_general | solution.py:164
  194.2 4.6 %fusion.86 = (f32[2,384]{1,0:T(2,128)S(1)}, f32[2,384,2048]{1,2,0:T(8,128)}) fusion(f32[2048,384,2]{1,0,2:T(8,128)S(1)} %fusion.85, bf16[2048,2,128]{0,2,1:T(8,128)(2,1)S(1)} %bitcast.68, bf16[384,2,128]{2,0,1:T(8,128)(2,1)S(1)} %get-tuple-element.326, pred[384,2048]{0,1:T(8,128)(4,1)S(1)} %broadcast_compare_fusion.2), kind=kOutput, calls=%fused_computation.75.clone.1 | convolution fusion | flops 408943872 | bytes 14617600 | tf_op jit(solution)/shard_map/while/body/eval_jaxpr/qhd,khd->hqk/dot_general | solution.py:151
  200.7 5.4 %fusion.90 = f32[384,2,128]{0,2,1:T(8,128)} fusion(bf16[2048,2,128]{0,2,1:T(8,128)(2,1)S(1)} %bitcast.69, f32[2,384,2048]{1,2,0:T(8,128)} %get-tuple-element.281, f32[2,384]{1,0:T(2,128)S(1)} %get-tuple-element.318, pred[384,2048]{0,1:T(8,128)(4,1)S(1)} %broadcast_compare_fusion.2, f32[384,2,128]{0,2,1:T(8,128)} %get-tuple-element.303, ...), kind=kOutput, calls=%fused_computation.14.clone.1 | convolution fusion | flops 407666688 | bytes 8919041 | tf_op jit(solution)/shard_map/while/body/eval_jaxpr/hqk,khd->qhd/dot_general | solution.py:164
  212.0 4.6 %fusion.86 = (f32[2,384]{1,0:T(2,128)S(1)}, f32[2,384,2048]{1,2,0:T(8,128)}) fusion(f32[2048,384,2]{1,0,2:T(8,128)S(1)} %fusion.85, bf16[2048,2,128]{0,2,1:T(8,128)(2,1)S(1)} %bitcast.68, bf16[384,2,128]{2,0,1:T(8,128)(2,1)S(1)} %get-tuple-element.326, pred[384,2048]{0,1:T(8,128)(4,1)S(1)} %broadcast_compare_fusion.2), kind=kOutput, calls=%fused_computation.75.clone.1 | convolution fusion | flops 408943872 | bytes 14617600 | tf_op jit(solution)/shard_map/while/body/eval_jaxpr/qhd,khd->hqk/dot_general | solution.py:151
  216.6 1.9 convolution_convert_fusion.6
  218.4 5.3 %fusion.90 = f32[384,2,128]{0,2,1:T(8,128)} fusion(bf16[2048,2,128]{0,2,1:T(8,128)(2,1)S(1)} %bitcast.69, f32[2,384,2048]{1,2,0:T(8,128)} %get-tuple-element.281, f32[2,384]{1,0:T(2,128)S(1)} %get-tuple-element.318, pred[384,2048]{0,1:T(8,128)(4,1)S(1)} %broadcast_compare_fusion.2, f32[384,2,128]{0,2,1:T(8,128)} %get-tuple-element.303, ...), kind=kOutput, calls=%fused_computation.14.clone.1 | convolution fusion | flops 407666688 | bytes 8919041 | tf_op jit(solution)/shard_map/while/body/eval_jaxpr/hqk,khd->qhd/dot_general | solution.py:164
  227.1 8.2 %all-to-all-start = ((bf16[8,48,256]{2,1,0:T(8,128)(2,1)}), bf16[8,48,256]{2,1,0:T(8,128)(2,1)S(1)}, u32[]{:S(2)}, u32[]{:S(2)}) async-start(bf16[8,48,256]{2,1,0:T(8,128)(2,1)} %all_to_all.20), calls=%async_computation | async-start | bytes 393216 | tf_op jit(solution)/shard_map/all_to_all | solution.py:203
  235.3 5.9 %all-to-all-done = bf16[8,48,256]{2,1,0:T(8,128)(2,1)S(1)} async-done(((bf16[8,48,256]{2,1,0:T(8,128)(2,1)}), bf16[8,48,256]{2,1,0:T(8,128)(2,1)S(1)}, u32[]{:S(2)}, u32[]{:S(2)}) %all-to-all-start) | async-done | bytes 196640 | tf_op jit(solution)/shard_map/all_to_all | solution.py:203
  241.2 5.2 %fusion.43 = (f32[48]{0:T(128)S(1)}, f32[48,2048]{1,0:T(8,128)S(1)}) fusion(bf16[48,2048]{1,0:T(8,128)(2,1)S(1)} %bitcast.75, bf16[2048,2048]{1,0:T(8,128)(2,1)} %param.28, bf16[384,2048]{1,0:T(8,128)(2,1)} %param.18, s32[]{:T(128)S(6)} %select_n.15), kind=kOutput, calls=%fused_computation.76 | convolution fusion | flops 403046336 | bytes 9175236 | tf_op jit(solution)/shard_map/dot_general | solution.py:204
  248.1 4.4 %all-to-all-start.1 = ((bf16[8,48,2048]{2,1,0:T(8,128)(2,1)}), bf16[8,48,2048]{2,1,0:T(8,128)(2,1)S(1)}, u32[]{:S(2)}, u32[]{:S(2)}) async-start(bf16[8,48,2048]{2,1,0:T(8,128)(2,1)} %broadcast_in_dim.34), calls=%async_computation.1 | async-start | bytes 3145728 | tf_op jit(solution)/shard_map/all_to_all | solution.py:35
  252.5 20.6 %all-to-all-done.1 = bf16[8,48,2048]{2,1,0:T(8,128)(2,1)S(1)} async-done(((bf16[8,48,2048]{2,1,0:T(8,128)(2,1)}), bf16[8,48,2048]{2,1,0:T(8,128)(2,1)S(1)}, u32[]{:S(2)}, u32[]{:S(2)}) %all-to-all-start.1) | async-done | bytes 1572896 | tf_op jit(solution)/shard_map/all_to_all | solution.py:35
  273.1 3.6 %fusion.44 = f32[384,704]{0,1:T(8,128)S(1)} fusion(bf16[384,2048]{1,0:T(8,128)(2,1)S(1)} %bitcast.72, bf16[2048,704]{1,0:T(8,128)(2,1)} %all-gather.8.cloned.1.call-done), kind=kOutput, calls=%fused_computation.77 | convolution fusion | flops 1107296256 | bytes 5537792 | tf_op jit(solution)/shard_map/dot_general | solution.py:210
  276.8 7.0 %convolution_convert_fusion.2 = bf16[384,2048]{1,0:T(8,128)(2,1)} fusion(bf16[704,2048]{0,1:T(8,128)(2,1)} %all-gather.12.cloned.1.call-done, bf16[384,2048]{1,0:T(8,128)(2,1)S(1)} %bitcast.73, bf16[2048,704]{1,0:T(8,128)(2,1)} %all-gather.10.cloned.1.call-done, f32[384,704]{0,1:T(8,128)S(1)} %fusion.44), kind=kOutput, calls=%fused_computation.32 | convolution fusion | flops 2217000960 | bytes 9994240 | tf_op jit(solution)/shard_map/dot_general | solution.py:213
  283.8 25.1 %all_to_all.29 = bf16[8,48,2048]{2,1,0:T(8,128)(2,1)S(1)} all-to-all(bf16[8,48,2048]{2,1,0:T(8,128)(2,1)} %bitcast.74), channel_id=1, replica_groups=mesh['sp_0'=8,'sp_1'=4,'tp'=8] {'tp'}, dimensions={0} | all-to-all | bytes 3145728 | tf_op jit(solution)/shard_map/all_to_all | solution.py:57
  (152 shorter events, 45.3 us)
Async XLA Ops:
  6.5 39.9 %copy-start = (bf16[512,384]{1,0:T(8,128)(2,1)S(1)}, bf16[512,384]{1,0:T(8,128)(2,1)}, u32[]{:S(2)}) copy-start(bf16[512,384]{1,0:T(8,128)(2,1)} %param.25) | copy-start | bytes 1179652
  6.5 28.4 %copy-start.5 = (bf16[704,64]{0,1:T(8,128)(2,1)S(1)}, bf16[704,64]{0,1:T(8,128)(2,1)}, u32[]{:S(2)}) copy-start(bf16[704,64]{0,1:T(8,128)(2,1)} %param.32) | copy-start | bytes 270340
  6.5 39.7 %copy-start.3 = (bf16[384,512]{1,0:T(8,128)(2,1)S(1)}, bf16[384,512]{1,0:T(8,128)(2,1)}, u32[]{:S(2)}) copy-start(bf16[384,512]{1,0:T(8,128)(2,1)} %param.19) | copy-start | bytes 1179652
  6.5 39.9 %copy-start.8 = (f32[512]{0:T(512)S(1)}, f32[512]{0:T(512)}, u32[]{:S(2)}) copy-start(f32[512]{0:T(512)} %param.23) | copy-start | bytes 6148
  6.5 104.4 %all-gather.6.cloned.1.call-start = ((), (), s32[]{:S(2)}) async-start(), calls=%async_computation.3 | async-start | bytes 8110080 | tf_op jit(solution)/shard_map/all_gather | solution.py:23
  9.5 37.7 %copy-start.6 = (s32[384]{0:T(512)S(1)}, s32[384]{0:T(512)}, u32[]{:S(2)}) copy-start(s32[384]{0:T(512)} %param.22) | copy-start | bytes 4612
  10.5 242.0 %all-gather.8.cloned.1.call-start = ((), (), s32[]{:S(2)}) async-start(), calls=%async_computation.4 | async-start | bytes 3538944 | tf_op jit(solution)/shard_map/all_gather | solution.py:45
  23.6 253.1 %all-gather.10.cloned.1.call-start = ((), (), s32[]{:S(2)}) async-start(), calls=%async_computation.5 | async-start | bytes 3538944 | tf_op jit(solution)/shard_map/all_gather | solution.py:45
  34.9 241.9 %all-gather.12.cloned.1.call-start = ((), (), s32[]{:S(2)}) async-start(), calls=%async_computation.6 | async-start | bytes 3538944 | tf_op jit(solution)/shard_map/all_gather | solution.py:45
  117.1 1.4 slice-start.2
  117.1 1.4 copy-start.1
  117.1 1.4 copy-start.2
  127.7 7.2 %slice-start = ((s8[6291456]{0:T(1024)(128)(4,1)}), s8[4194304]{0:T(1024)(128)(4,1)S(1)}, s32[]{:S(2)}) async-start(s8[6291456]{0:T(1024)(128)(4,1)} %bitcast.66), calls=%async_computation.7 | async-start | bytes 8388608 | tf_op jit(solution)/shard_map/while
  129.6 5.3 %slice-start.1 = ((s8[6291456]{0:T(1024)(128)(4,1)}), s8[2097152]{0:T(1024)(128)(4,1)S(1)}, s32[]{:S(2)}) async-start(s8[6291456]{0:T(1024)(128)(4,1)} %bitcast.66), calls=%async_computation.8 | async-start | bytes 4194304 | tf_op jit(solution)/shard_map/while
  145.4 7.3 %slice-start = ((s8[6291456]{0:T(1024)(128)(4,1)}), s8[4194304]{0:T(1024)(128)(4,1)S(1)}, s32[]{:S(2)}) async-start(s8[6291456]{0:T(1024)(128)(4,1)} %bitcast.66), calls=%async_computation.7 | async-start | bytes 8388608 | tf_op jit(solution)/shard_map/while
  147.3 5.4 %slice-start.1 = ((s8[6291456]{0:T(1024)(128)(4,1)}), s8[2097152]{0:T(1024)(128)(4,1)S(1)}, s32[]{:S(2)}) async-start(s8[6291456]{0:T(1024)(128)(4,1)} %bitcast.66), calls=%async_computation.8 | async-start | bytes 4194304 | tf_op jit(solution)/shard_map/while
  163.2 7.2 %slice-start = ((s8[6291456]{0:T(1024)(128)(4,1)}), s8[4194304]{0:T(1024)(128)(4,1)S(1)}, s32[]{:S(2)}) async-start(s8[6291456]{0:T(1024)(128)(4,1)} %bitcast.66), calls=%async_computation.7 | async-start | bytes 8388608 | tf_op jit(solution)/shard_map/while
  165.1 5.3 %slice-start.1 = ((s8[6291456]{0:T(1024)(128)(4,1)}), s8[2097152]{0:T(1024)(128)(4,1)S(1)}, s32[]{:S(2)}) async-start(s8[6291456]{0:T(1024)(128)(4,1)} %bitcast.66), calls=%async_computation.8 | async-start | bytes 4194304 | tf_op jit(solution)/shard_map/while
  181.0 7.3 %slice-start = ((s8[6291456]{0:T(1024)(128)(4,1)}), s8[4194304]{0:T(1024)(128)(4,1)S(1)}, s32[]{:S(2)}) async-start(s8[6291456]{0:T(1024)(128)(4,1)} %bitcast.66), calls=%async_computation.7 | async-start | bytes 8388608 | tf_op jit(solution)/shard_map/while
  182.9 5.4 %slice-start.1 = ((s8[6291456]{0:T(1024)(128)(4,1)}), s8[2097152]{0:T(1024)(128)(4,1)S(1)}, s32[]{:S(2)}) async-start(s8[6291456]{0:T(1024)(128)(4,1)} %bitcast.66), calls=%async_computation.8 | async-start | bytes 4194304 | tf_op jit(solution)/shard_map/while
  198.8 7.2 %slice-start = ((s8[6291456]{0:T(1024)(128)(4,1)}), s8[4194304]{0:T(1024)(128)(4,1)S(1)}, s32[]{:S(2)}) async-start(s8[6291456]{0:T(1024)(128)(4,1)} %bitcast.66), calls=%async_computation.7 | async-start | bytes 8388608 | tf_op jit(solution)/shard_map/while
  200.7 5.4 %slice-start.1 = ((s8[6291456]{0:T(1024)(128)(4,1)}), s8[2097152]{0:T(1024)(128)(4,1)S(1)}, s32[]{:S(2)}) async-start(s8[6291456]{0:T(1024)(128)(4,1)} %bitcast.66), calls=%async_computation.8 | async-start | bytes 4194304 | tf_op jit(solution)/shard_map/while
  216.6 7.2 %slice-start = ((s8[6291456]{0:T(1024)(128)(4,1)}), s8[4194304]{0:T(1024)(128)(4,1)S(1)}, s32[]{:S(2)}) async-start(s8[6291456]{0:T(1024)(128)(4,1)} %bitcast.66), calls=%async_computation.7 | async-start | bytes 8388608 | tf_op jit(solution)/shard_map/while
  218.4 5.3 %slice-start.1 = ((s8[6291456]{0:T(1024)(128)(4,1)}), s8[2097152]{0:T(1024)(128)(4,1)S(1)}, s32[]{:S(2)}) async-start(s8[6291456]{0:T(1024)(128)(4,1)} %bitcast.66), calls=%async_computation.8 | async-start | bytes 4194304 | tf_op jit(solution)/shard_map/while
  227.1 14.1 %all-to-all-start = ((bf16[8,48,256]{2,1,0:T(8,128)(2,1)}), bf16[8,48,256]{2,1,0:T(8,128)(2,1)S(1)}, u32[]{:S(2)}, u32[]{:S(2)}) async-start(bf16[8,48,256]{2,1,0:T(8,128)(2,1)} %all_to_all.20), calls=%async_computation | async-start | bytes 393216 | tf_op jit(solution)/shard_map/all_to_all | solution.py:203
  241.2 5.4 %copy-start.4 = (f32[2048]{0:T(1024)S(1)}, f32[2048]{0:T(1024)}, u32[]{:S(2)}) copy-start(f32[2048]{0:T(1024)} %param.29) | copy-start | bytes 24580
  248.1 25.0 %all-to-all-start.1 = ((bf16[8,48,2048]{2,1,0:T(8,128)(2,1)}), bf16[8,48,2048]{2,1,0:T(8,128)(2,1)S(1)}, u32[]{:S(2)}, u32[]{:S(2)}) async-start(bf16[8,48,2048]{2,1,0:T(8,128)(2,1)} %broadcast_in_dim.34), calls=%async_computation.1 | async-start | bytes 3145728 | tf_op jit(solution)/shard_map/all_to_all | solution.py:35
  283.8 25.9 %copy-start.7 = (f32[2048]{0:T(1024)S(1)}, f32[2048]{0:T(1024)}, u32[]{:S(2)}) copy-start(f32[2048]{0:T(1024)} %param.33) | copy-start | bytes 24580
Sparse Core Ops, SparseCore 0:
  10.6 100.2 all-gather.5
  112.7 47.6 all-gather.7
  162.2 43.5 all-gather.9
  207.5 43.5 all-gather.11
where the time goes:
time: 318 us; the launch traced here: 317 us
  blocking collectives  103 us (32%)
  matrix products  103 us (32%)
  waiting for transfers between devices  48.3 us (15%)
  other arithmetic  17.4 us (5%)
  local copies, waits for them, and re-layouts  15 us (5%)
  between operations  13.4 us (4%)
  starting transfers between devices  12.7 us (4%)
  loops' own time  4.29 us (1%)
    all_gather x1, blocking collectives, body(): lax.all_gather(doc_ids, SP, axis=0, tiled=True)  42.1 us
    all_gather x3, blocking collectives, gather_axes(): whole = lax.all_gather(whole, axes[number], axis=dim, tiled=True)  35.5 us
    dot_general x6, matrix products, attend_rows(): jnp.einsum('hqk,khd->qhd', weights.astype(jnp.bfloat16), values_heads, pr...  32 us
    dot_general x6, matrix products, attend_rows(): jnp.einsum('qhd,khd->hqk', query_nope, keys_heads, preferred_element_type...  27.5 us
    all_to_all x1, blocking collectives, sent_and_summed(): tiles = lax.all_to_all(in_blocks(value, dim, count), axis, 0, 0, tiled=True)  25.1 us
    all_gather x1, waiting for transfers between devices, sent_together(): whole = lax.all_gather(both, axis, axis=dim, tiled=True)  21.7 us
    all_to_all x1, waiting for transfers between devices, copy_for_each(): return lax.all_to_all(copies, axis, split_axis=0, concat_axis=0, tiled=True)  20.6 us
    dot_general x6, matrix products, project_rows(): jnp.dot(latent_piece, w_value, preferred_element_type=jnp.float32)  11.2 us
  transfers between devices with their start and end apart: 6, of which 3 were waited for; matrix products, arithmetic and copies ran while one was open for 38% of the time, Pallas kernels for 0%

commit v1 on v0

v1 whole, which is shorter than its diff:
```python
import functools
import math

import jax
import jax.numpy as jnp
from jax import lax
from jax.experimental import pallas as pl
from jax.experimental.pallas import tpu as pltpu
from jax.sharding import Mesh
from jax.sharding import PartitionSpec as P

NOPE = 128
RD = 64
VD = 128
NZ, NY, NX, NC = 8, 4, 4, 2
SP = ("z", "y")
TP = ("x", "c")
MESH = pl.DeviceIdType.MESH

eps_norm = 1e-05
rope_theta = 10000.0
resid_alpha = 8.0**0.25
HEADS_DEV = 2
WIDE = 384
QUART = 96
EXP2_SCALE = (NOPE + RD) ** (-0.5) * math.log2(math.e)
F32 = jnp.float32
BF16 = jnp.bfloat16


def rope_angles(positions):
    frequency = rope_theta ** (-jnp.arange(0, RD, 2, dtype=jnp.float32) / RD)
    angles = positions.astype(jnp.float32)[:, None] * frequency[None, :]
    return (jnp.cos(angles), jnp.sin(angles))


def rotate(values, cos_table, sin_table):
    half_width = values.shape[-1] // 2
    first_half = values[..., :half_width]
    second_half = values[..., half_width:]
    return jnp.concatenate(
        [
            first_half * cos_table - second_half * sin_table,
            second_half * cos_table + first_half * sin_table,
        ],
        axis=-1,
    )


def rms_scaled(latent, scaling):
    widened = latent.astype(jnp.float32)
    inverse = lax.rsqrt(jnp.mean(widened * widened, axis=-1, keepdims=True) + eps_norm)
    return (widened * inverse * scaling).astype(jnp.bfloat16)


def layer_scaled(stream, scaling):
    centre = stream - jnp.mean(stream, axis=-1, keepdims=True)
    spread = jnp.mean(centre * centre, axis=-1, keepdims=True)
    return centre * lax.rsqrt(spread + eps_norm) * scaling


class Wires:
    def __init__(self):
        self.sent = []

    def copy(self, slot, pair, index, axis, target):
        send, recv = pair
        ref = slot()
        return pltpu.make_async_remote_copy(
            src_ref=ref,
            dst_ref=ref,
            send_sem=send.at[index],
            recv_sem=recv.at[index],
            device_id={axis: target},
            device_id_type=MESH,
        )

    def start(self, slot, pair, index, axis, target):
        self.copy(slot, pair, index, axis, target).start()
        self.sent.append((slot, pair, index, axis, target))

    def landed(self, slot, pair, index, axis, target):
        self.copy(slot, pair, index, axis, target).wait_recv()

    def finish(self):
        for item in self.sent:
            self.copy(*item).wait_send()


class RingYZ:
    SEMS = 12

    def __init__(self, wires, at, chunk, part, pair, me):
        self.w, self.at, self.chunk, self.part, self.pair = wires, at, chunk, part, pair
        z, y = me
        self.y = y
        self.yl, self.yr, self.yo = (y + 3) % 4, (y + 1) % 4, (y + 2) % 4
        self.zz = [lax.rem(z + d, 8) for d in range(8)]
        self.z = z

    def send(self, slot, index, axis, target):
        self.w.start(slot, self.pair, index, axis, target)

    def got(self, slot, index, axis="y"):
        target = self.yr if axis == "y" else self.zz[1]
        self.w.landed(slot, self.pair, index, axis, target)

    def y1(self):
        own = lambda: self.at(self.z, self.y)
        self.send(own, 0, "y", self.yr)
        self.send(own, 1, "y", self.yl)

    def y2(self):
        self.got(lambda: self.at(self.z, self.yl), 0)
        self.got(lambda: self.at(self.z, self.yr), 1)
        self.send(lambda: self.part(self.z, self.yl, 0), 2, "y", self.yr)
        self.send(lambda: self.part(self.z, self.yr, 1), 3, "y", self.yl)

    def z1(self):
        self.got(lambda: self.part(self.z, self.yo, 0), 2)
        self.got(lambda: self.part(self.z, self.yo, 1), 3)
        self.send(lambda: self.chunk(self.z, 0, 4), 4, "z", self.zz[1])
        self.send(lambda: self.chunk(self.z, 0, 4), 8, "z", self.zz[7])

    def zs(self, s):
        right, left = self.zz[9 - s], self.zz[s - 1]
        self.got(lambda: self.chunk(right, 0, 4), 4 + s - 2, "z")
        self.got(lambda: self.chunk(left, 0, 4), 8 + s - 2, "z")
        if s < 4:
            self.send(lambda: self.chunk(right, 0, 4), 4 + s - 1, "z", self.zz[1])
            self.send(lambda: self.chunk(left, 0, 4), 8 + s - 1, "z", self.zz[7])
        else:
            self.send(lambda: self.chunk(right, 0, 2), 7, "z", self.zz[1])
            self.send(lambda: self.chunk(left, 2, 4), 11, "z", self.zz[7])

    def z5(self):
        self.got(lambda: self.chunk(self.zz[4], 0, 2), 7, "z")
        self.got(lambda: self.chunk(self.zz[4], 2, 4), 11, "z")


class RingZY:
    SEMS = 40

    def __init__(self, wires, at, part, pair, me):
        self.w, self.at, self.part, self.pair = wires, at, part, pair
        z, y = me
        self.y = y
        self.yl, self.yr, self.yo = (y + 3) % 4, (y + 1) % 4, (y + 2) % 4
        self.zz = [lax.rem(z + d, 8) for d in range(8)]
        self.z = z

    def send(self, slot, index, axis, target):
        self.w.start(slot, self.pair, index, axis, target)

    def got(self, slot, index, axis):
        target = self.yr if axis == "y" else self.zz[1]
        self.w.landed(slot, self.pair, index, axis, target)

    def z1(self):
        own = lambda: self.at(self.z, self.y)
        self.send(own, 0, "z", self.zz[1])
        self.send(own, 4, "z", self.zz[7])

    def zs(self, s):
        right, left = self.zz[9 - s], self.zz[s - 1]
        self.got(lambda: self.at(right, self.y), s - 2, "z")
        self.got(lambda: self.at(left, self.y), 4 + s - 2, "z")
        if s < 4:
            self.send(lambda: self.at(right, self.y), s - 1, "z", self.zz[1])
            self.send(lambda: self.at(left, self.y), 4 + s - 1, "z", self.zz[7])
        else:
            self.send(lambda: self.part(right, self.y, 0), 3, "z", self.zz[1])
            self.send(lambda: self.part(left, self.y, 1), 7, "z", self.zz[7])

    def z5(self):
        self.got(lambda: self.part(self.zz[4], self.y, 0), 3, "z")
        self.got(lambda: self.part(self.zz[4], self.y, 1), 7, "z")

    def y1(self, d):
        zz = self.zz[d]
        self.send(lambda: self.at(zz, self.y), 8 + 4 * d, "y", self.yr)
        self.send(lambda: self.at(zz, self.y), 9 + 4 * d, "y", self.yl)

    def y2(self, d):
        zz = self.zz[d]
        self.got(lambda: self.at(zz, self.yl), 8 + 4 * d, "y")
        self.got(lambda: self.at(zz, self.yr), 9 + 4 * d, "y")
        self.send(lambda: self.part(zz, self.yl, 0), 10 + 4 * d, "y", self.yr)
        self.send(lambda: self.part(zz, self.yr, 1), 11 + 4 * d, "y", self.yl)

    def y3(self, d):
        zz = self.zz[d]
        self.got(lambda: self.part(zz, self.yo, 0), 10 + 4 * d, "y")
        self.got(lambda: self.part(zz, self.yo, 1), 11 + 4 * d, "y")


def layer_kernel(
    q_ref,
    kvm_ref,
    wg_ref,
    wu_ref,
    wd_ref,
    wkv_ref,
    att_ref,
    wa_out,
    wb_out,
    kv,
    wa,
    wb,
    m_ref,
    l_ref,
    acc_ref,
    loc_sem,
    ka_s,
    ka_r,
    kb_s,
    kb_r,
    kp_s,
    kp_r,
    wa_s,
    wa_r,
    wb_s,
    wb_r,
):
    z, y, c = lax.axis_index("z"), lax.axis_index("y"), lax.axis_index("c")
    other = 1 - c
    zz = [lax.rem(z + d, 8) for d in range(8)]

    own_rows = pl.multiple_of(c * 192, 96)
    local = [
        pltpu.make_async_copy(kvm_ref.at[pl.ds(own_rows, 96)], kv.at[0, c, z, y], loc_sem.at[0]),
        pltpu.make_async_copy(
            kvm_ref.at[pl.ds(own_rows + 96, 96)], kv.at[1, c, z, y], loc_sem.at[1]
        ),
        pltpu.make_async_copy(wg_ref, wa.at[z, y], loc_sem.at[2]),
        pltpu.make_async_copy(wu_ref, wb.at[z, y, 0], loc_sem.at[3]),
        pltpu.make_async_copy(wd_ref, wb.at[z, y, 1], loc_sem.at[4]),
    ]
    for copy in local:
        copy.start()

    barrier = pltpu.get_barrier_semaphore()
    for axis, target in (
        ("z", zz[1]),
        ("z", zz[7]),
        ("y", (y + 1) % 4),
        ("y", (y + 3) % 4),
        ("c", other),
    ):
        pl.semaphore_signal(barrier, inc=1, device_id={axis: target}, device_id_type=MESH)

    m_ref[...] = jnp.full(m_ref.shape, -1e30, F32)
    l_ref[...] = jnp.zeros(l_ref.shape, F32)
    acc_ref[...] = jnp.zeros(acc_ref.shape, F32)
    for copy in local:
        copy.wait()
    pl.semaphore_wait(barrier, 5)

    wires = Wires()
    half = lambda h: pl.ds(48 * h, 48)
    ka = RingYZ(
        wires,
        lambda a, b: kv.at[0, c, a, b],
        lambda a, lo, hi: kv.at[0, c, a, pl.ds(lo, hi - lo)],
        lambda a, b, h: kv.at[0, c, a, b, half(h)],
        (ka_s, ka_r),
        (z, y),
    )
    kb = RingZY(
        wires,
        lambda a, b: kv.at[1, c, a, b],
        lambda a, b, h: kv.at[1, c, a, b, half(h)],
        (kb_s, kb_r),
        (z, y),
    )
    ga = RingYZ(
        wires,
        lambda a, b: wa.at[a, b],
        lambda a, lo, hi: wa.at[a, pl.ds(lo, hi - lo)],
        lambda a, b, h: wa.at[a, b, pl.ds(32 * h, 32)],
        (wa_s, wa_r),
        (z, y),
    )
    gb = RingZY(
        wires,
        lambda a, b: wb.at[a, b],
        lambda a, b, h: wb.at[a, b, h],
        (wb_s, wb_r),
        (z, y),
    )

    def to_core(color, d):
        wires.start(lambda: kv.at[color, c, zz[d]], (kp_s, kp_r), 8 * color + d, "c", other)

    def attend(u):
        v = u + 2
        rnd, w = v // 4, v % 4
        color = w % 2
        d = lax.rem(jnp.where(w < 2, rnd, 8 - rnd), 8)
        at_z = lax.rem(z + d, 8)
        wires.landed(
            lambda: kv.at[color, other, at_z], (kp_s, kp_r), 8 * color + d, "c", other
        )
        x = kv[color, :, at_z].reshape(768, WIDE)
        extra = x[:, 256:384]
        both = jnp.dot(x[:, :256], wkv_ref[...], preferred_element_type=F32).astype(BF16)
        for h in range(HEADS_DEV):
            keys = jnp.concatenate([both[:, 128 * h : 128 * h + 128], extra], axis=1)
            vals = both[:, 256 + 128 * h : 384 + 128 * h]
            s = lax.dot_general(
                q_ref[h], keys, (((1,), (1,)), ((), ())), preferred_element_type=F32
            )
            top_old = m_ref[h]
            top = jnp.maximum(top_old, jnp.max(s, axis=1, keepdims=True))
            factor = jnp.exp2((top_old - top) * EXP2_SCALE)
            p = jnp.exp2((s - jnp.concatenate([top] * 6, axis=1)) * EXP2_SCALE)
            part = p[:, :128]
            for k in range(1, 6):
                part = part + p[:, 128 * k : 128 * k + 128]
            m_ref[h] = top
            l_ref[h] = l_ref[h] * factor + part
            acc_ref[h] = acc_ref[h] * factor + jnp.dot(
                p.astype(BF16), vals, preferred_element_type=F32
            )

    ka.y1()
    kb.z1()
    kb.y1(0)
    ka.y2()
    kb.zs(2)
    kb.y1(1)
    kb.y1(7)
    ka.z1()
    to_core(0, 0)
    kb.y2(0)
    kb.zs(3)
    kb.y1(2)
    kb.y1(6)
    kb.y3(0)
    to_core(1, 0)
    kb.y2(1)
    kb.y2(7)

    def event(u):
        if u == 2:
            kb.zs(4)
            kb.y1(3)
            kb.y1(5)
            ka.zs(2)
            to_core(0, 1)
            to_core(0, 7)
            kb.z5()
            kb.y1(4)
            kb.y3(1)
            kb.y3(7)
            to_core(1, 1)
            to_core(1, 7)
            kb.y2(2)
            kb.y2(6)
            ga.y1()
            gb.z1()
        if u == 6:
            ka.zs(3)
            to_core(0, 2)
            to_core(0, 6)
            kb.y3(2)
            kb.y3(6)
            to_core(1, 2)
            to_core(1, 6)
            kb.y2(3)
            kb.y2(5)
            ga.y2()
            gb.zs(2)
            gb.y1(0)
        if u == 10:
            ka.zs(4)
            to_core(0, 3)
            to_core(0, 5)
            kb.y3(3)
            kb.y3(5)
            to_core(1, 3)
            to_core(1, 5)
            kb.y2(4)
            ga.z1()
            gb.zs(3)
            gb.y1(1)
            gb.y1(7)
        if u == 14:
            ka.z5()
            to_core(0, 4)
            kb.y3(4)
            to_core(1, 4)
            gb.y2(0)
            gb.zs(4)
            gb.y1(2)
            gb.y1(6)

    def step(u, carry):
        for k in (2, 6, 10, 14):

            @pl.when(u == k)
            def _():
                event(k)

        attend(u)
        return carry

    lax.fori_loop(0, 16, step, 0)

    for h in range(HEADS_DEV):
        denom = jnp.sum(l_ref[h], axis=1, keepdims=True)
        att_ref[:, 128 * h : 128 * h + 128] = (acc_ref[h] / denom).astype(BF16)

    gb.z5()
    gb.y1(3)
    gb.y1(5)
    gb.y2(1)
    gb.y2(7)
    gb.y3(0)
    ga.zs(2)
    gb.y1(4)
    gb.y2(2)
    gb.y2(6)
    gb.y3(1)
    gb.y3(7)
    ga.zs(3)
    gb.y2(3)
    gb.y2(5)
    gb.y3(2)
    gb.y3(6)
    gb.y2(4)
    ga.zs(4)
    gb.y3(3)
    gb.y3(5)
    gb.y3(4)
    ga.z5()
    outs = [
        pltpu.make_async_copy(wa, wa_out, loc_sem.at[0]),
        pltpu.make_async_copy(wb, wb_out, loc_sem.at[1]),
    ]
    for copy in outs:
        copy.start()
    wires.finish()
    for copy in outs:
        copy.wait()


def body(
    resid_stream,
    q_latent,
    kv_latent,
    rope_key,
    doc_ids,
    q_gain,
    kv_gain,
    w_query,
    w_key,
    w_value,
    w_out,
    mix_gain,
    w_gate,
    w_up,
    w_down,
    out_gain,
):
    tok_rows = q_latent.shape[0]
    part_rows = tok_rows // (NX * NC)
    tp_index = lax.axis_index(TP)
    positions = lax.axis_index(SP) * tok_rows + jnp.arange(tok_rows, dtype=jnp.int32)
    cos_table, sin_table = rope_angles(positions)
    q_normed = rms_scaled(q_latent, q_gain)
    queries = jnp.dot(q_normed, w_query, preferred_element_type=jnp.float32).reshape(
        tok_rows, HEADS_DEV, NOPE + RD
    )
    kv_normed = rms_scaled(kv_latent, kv_gain)
    key_rot = rotate(rope_key.astype(jnp.float32), cos_table, sin_table).astype(jnp.bfloat16)
    slots = jnp.arange(64, dtype=jnp.int32)
    same = doc_ids[:, None] == slots[None, :]
    message = jnp.concatenate([kv_normed, key_rot, same.astype(BF16)], axis=1)
    apart = jnp.where(same | (slots >= 4)[None, :], 0.0, -1e30).astype(BF16)
    q_heads = []
    for h in range(HEADS_DEV):
        q_heads.append(
            jnp.concatenate(
                [
                    queries[:, h, :NOPE].astype(BF16),
                    rotate(queries[:, h, NOPE:], cos_table, sin_table).astype(BF16),
                    apart,
                ],
                axis=1,
            )
        )
    q_all = jnp.stack(q_heads)
    wkv = jnp.concatenate([w_key, w_value], axis=1)

    any_spec = pl.BlockSpec(memory_space=pl.ANY)
    vmem_spec = pl.BlockSpec(memory_space=pltpu.VMEM)
    dma = pltpu.SemaphoreType.DMA
    attended, wa, wb = pl.pallas_call(
        layer_kernel,
        out_shape=(
            jax.ShapeDtypeStruct((tok_rows, HEADS_DEV * VD), BF16),
            jax.ShapeDtypeStruct((NZ, NY, 64, 704), BF16),
            jax.ShapeDtypeStruct((NZ, NY, 2, 64, 704), BF16),
        ),
        in_specs=[vmem_spec, any_spec, any_spec, any_spec, any_spec, vmem_spec],
        out_specs=(vmem_spec, any_spec, any_spec),
        scratch_shapes=[
            pltpu.VMEM((2, NC, NZ, NY, QUART, WIDE), BF16),
            pltpu.VMEM((NZ, NY, 64, 704), BF16),
            pltpu.VMEM((NZ, NY, 2, 64, 704), BF16),
            pltpu.VMEM((HEADS_DEV, tok_rows, 128), F32),
            pltpu.VMEM((HEADS_DEV, tok_rows, 128), F32),
            pltpu.VMEM((HEADS_DEV, tok_rows, 128), F32),
            dma((8,)),
            dma((12,)),
            dma((12,)),
            dma((40,)),
            dma((40,)),
            dma((16,)),
            dma((16,)),
            dma((12,)),
            dma((12,)),
            dma((40,)),
            dma((40,)),
        ],
        compiler_params=pltpu.CompilerParams(
            collective_id=0, has_side_effects=True, vmem_limit_bytes=60 * 1024 * 1024
        ),
        name="gather_attend",
    )(q_all, message, w_gate, w_up, w_down.T, wkv)

    wg_all = wa.reshape(2048, 704)
    wu_all = wb[:, :, 0].reshape(2048, 704)
    wd_all = wb[:, :, 1].reshape(2048, 704)

    heads_rows = lax.all_to_all(attended, TP, split_axis=0, concat_axis=1, tiled=True)
    mixer_out = jnp.dot(heads_rows, w_out, preferred_element_type=jnp.float32)
    own_resid = lax.dynamic_slice_in_dim(resid_stream, tp_index * part_rows, part_rows, 0)
    own_normed = layer_scaled(
        resid_alpha * own_resid.astype(jnp.float32) + mixer_out, mix_gain
    ).astype(jnp.bfloat16)
    copies = jnp.broadcast_to(own_normed, (8, *own_normed.shape))
    normed_rows = lax.all_to_all(copies, TP, split_axis=0, concat_axis=0, tiled=True).reshape(
        tok_rows, 2048
    )
    gate_part = jnp.dot(normed_rows, wg_all, preferred_element_type=jnp.float32)
    up_part = jnp.dot(normed_rows, wu_all, preferred_element_type=jnp.float32)
    hidden = (jax.nn.silu(gate_part) * up_part).astype(jnp.bfloat16)
    down_term = lax.dot_general(
        hidden, wd_all, (((1,), (1,)), ((), ())), preferred_element_type=jnp.float32
    )
    tiles = lax.all_to_all(
        down_term.astype(BF16).reshape(8, part_rows, 2048), TP, 0, 0, tiled=True
    )
    ffn_sum = jnp.sum(tiles.astype(jnp.float32), axis=0)
    layer_out = layer_scaled(
        resid_alpha * own_normed.astype(jnp.float32) + 0.5 * ffn_sum, out_gain
    ).astype(jnp.bfloat16)
    return layer_out


def solution(mesh):
    split = Mesh(mesh.devices.reshape(NZ, NY, NX, NC), ("z", "y", "x", "c"))
    in_specs = (
        P(SP, None),
        P(SP, None),
        P(SP, None),
        P(SP, None),
        P(SP),
        P(),
        P(),
        P(None, TP),
        P(None, TP),
        P(None, TP),
        P(),
        P(),
        P(SP, TP),
        P(SP, TP),
        P(TP, SP),
        P(),
    )
    out_specs = P((*SP, *TP), None)
    return jax.shard_map(body, mesh=split, in_specs=in_specs, out_specs=out_specs, check_vma=False)
```

time: 318 us -> 197 us (0.62)
  Pallas kernels: 0 us -> 107 us
  matrix products: 103 us -> 17.2 us
  blocking collectives: 103 us -> 25 us
  waiting for transfers between devices: 48.3 us -> 20.2 us
  between operations: 13.4 us -> 0.28 us
  other arithmetic: 17.4 us -> 7.3 us
  local copies, waits for them, and re-layouts: 15 us -> 8.6 us
  loops' own time: 4.29 us -> 0 us
    pallas_call x0 -> x1, Pallas kernels: none -> 107 us  [body(): pl.pallas_call(layer_kernel, out_shape=(jax.ShapeDtypeStruct((tok_rows, H...]
    dot_general x32 -> x2, matrix products: 97.8 us -> 10.6 us  [the longest x1 7.04 us: body(): lax.dot_general(hidden, wd_all, (((1,), (1,)), ((), ())), preferred_eleme...]
    all_gather x4 -> x0, blocking collectives: 77.6 us -> none  [the longest x1 42.1 us: body(): lax.all_gather(doc_ids, SP, axis=0, tiled=True)]
    all_gather x4 -> x0, waiting for transfers between devices: 21.7 us -> none  [the longest x1 21.7 us: sent_together(): whole = lax.all_gather(both, axis, axis=dim, tiled=True)]
    reduce_sum x7 -> x1, other arithmetic: 7.85 us -> 0.23 us  [body(): ffn_sum = jnp.sum(tiles.astype(jnp.float32), axis=0)]
    split x3 -> x0, local copies, waits for them, and re-layouts: 7.53 us -> none  [sent_together(): jnp.split(whole, [sum(widths[:k]) for k in range(1, len(widths))], axis=a...]
    all_to_all x2, waiting for transfers between devices: 26.5 us -> 20.2 us  [the longest x1 14.3 us: body(): lax.all_to_all(copies, TP, split_axis=0, concat_axis=0, tiled=True)]
    slice x1, local copies, waits for them, and re-layouts: 0.02 us -> 6.29 us  [body(): wu_all = wb[:, :, 0].reshape(2048, 704)]
  transfers between devices with their start and end apart: 6 -> 2, of which waited for: 3 -> 2; matrix products, arithmetic and copies ran while one was open for 38% -> 3% of each run, Pallas kernels for 0% -> 0%
where the time goes in v1:
time: 197 us
  Pallas kernels  107 us (54%)
  blocking collectives  25 us (13%)
  waiting for transfers between devices  20.2 us (10%)
  matrix products  17.2 us (9%)
  starting transfers between devices  10.9 us (6%)
  local copies, waits for them, and re-layouts  8.6 us (4%)
  other arithmetic  7.3 us (4%)
    pallas_call x1, Pallas kernels, body(): pl.pallas_call(layer_kernel, out_shape=(jax.ShapeDtypeStruct((tok_rows, H...  107 us
    all_to_all x1, blocking collectives, body(): lax.all_to_all(down_term.astype(BF16).reshape(8, part_rows, 2048), TP, 0,...  25 us
    all_to_all x1, waiting for transfers between devices, body(): lax.all_to_all(copies, TP, split_axis=0, concat_axis=0, tiled=True)  14.3 us
    dot_general x1, matrix products, body(): lax.dot_general(hidden, wd_all, (((1,), (1,)), ((), ())), preferred_eleme...  7.04 us
    all_to_all x1, starting transfers between devices, body(): lax.all_to_all(attended, TP, split_axis=0, concat_axis=1, tiled=True)  6.43 us
    slice x1, local copies, waits for them, and re-layouts, body(): wu_all = wb[:, :, 0].reshape(2048, 704)  6.29 us
    all_to_all x1, waiting for transfers between devices, body(): lax.all_to_all(attended, TP, split_axis=0, concat_axis=1, tiled=True)  5.86 us
    dot_general x1, matrix products, body(): mixer_out = jnp.dot(heads_rows, w_out, preferred_element_type=jnp.float32)  5.08 us
  transfers between devices with their start and end apart: 2, of which 2 were waited for; matrix products, arithmetic and copies ran while one was open for 3% of the time, Pallas kernels for 0%

profile of v1, /device:TPU:1, one launch (start us, length us, event | category | flops | bytes accessed | tf_op | source)
XLA Modules:
  0.0 196.7 jit_solution(6332175638230631088)
XLA Ops:
  0.0 1.2 fusion.1
  1.2 1.5 fusion.8
  2.7 0.0 copy-start.1
  2.8 0.3 copy.28
  3.2 0.5 copy-done.1
  3.7 0.1 fusion.5
  3.8 0.1 fusion.38
  4.0 0.1 select_convert_fusion
  4.1 0.1 copy.32
  4.3 0.1 fusion.7
  4.4 0.7 pad_maximum_fusion.2.wkv_ref
  5.2 0.9 fusion.35
  6.1 0.2 fusion.24
  6.3 0.8 pad_maximum_fusion.q_ref
  7.0 0.8 pad_maximum_fusion.1.kvm_ref
  7.9 107.2 %gather_attend.1 = (bf16[384,256]{1,0:T(8,128)(2,1)}, bf16[8,4,64,704]{3,2,1,0:T(8,128)(2,1)}, bf16[8,4,2,64,704]{4,3,2,1,0:T(8,128)(2,1)}) custom-call(bf16[2,384,256]{2,1,0:T(8,128)(2,1)} %pad_maximum_fusion.q_ref, bf16[384,384]{1,0:T(8,128)(2,1)} %pad_maximum_fusion.1.kvm_ref, bf16[64,704]{1,0:T(8,128)(2,1)} %wg_ref.1, bf16[64,704]{1,0:T(8,128)(2,1)} %wu_ref.1, ...), custom_call_target="tpu_custom_call" | custom-call | tf_op jit(solution)/shard_map/gather_attend/pallas_call | solution.py:499
  115.1 6.4 %all-to-all-start = ((bf16[8,48,256]{2,1,0:T(8,128)(2,1)}), bf16[8,48,256]{2,1,0:T(8,128)(2,1)S(1)}, u32[]{:S(2)}, u32[]{:S(2)}) async-start(bf16[8,48,256]{2,1,0:T(8,128)(2,1)} %bitcast.39), calls=%async_computation | async-start | bytes 393216 | tf_op jit(solution)/shard_map/all_to_all | solution.py:537
  121.5 5.9 %all-to-all-done = bf16[8,48,256]{2,1,0:T(8,128)(2,1)S(1)} async-done(((bf16[8,48,256]{2,1,0:T(8,128)(2,1)}), bf16[8,48,256]{2,1,0:T(8,128)(2,1)S(1)}, u32[]{:S(2)}, u32[]{:S(2)}) %all-to-all-start) | async-done | bytes 196640 | tf_op jit(solution)/shard_map/all_to_all | solution.py:537
  127.4 5.1 %fusion.43 = (f32[48]{0:T(128)S(1)}, f32[48,2048]{1,0:T(8,128)S(1)}) fusion(bf16[48,2048]{1,0:T(8,128)(2,1)S(1)} %bitcast.37, bf16[2048,2048]{1,0:T(8,128)(2,1)} %param.26, bf16[384,2048]{1,0:T(8,128)(2,1)} %param.16, s32[]{:T(128)S(6)} %select_n.7), kind=kOutput, calls=%fused_computation.77 | convolution fusion | flops 403046336 | bytes 9175236 | tf_op jit(solution)/shard_map/dot_general | solution.py:538
  132.5 0.2 multiply_reduce_fusion.1
  132.8 0.1 multiply_convert_fusion.1
  132.9 1.3 broadcast_in_dim.10
  134.2 4.4 %all-to-all-start.1 = ((bf16[8,48,2048]{2,1,0:T(8,128)(2,1)}), bf16[8,48,2048]{2,1,0:T(8,128)(2,1)S(1)}, u32[]{:S(2)}, u32[]{:S(2)}) async-start(bf16[8,48,2048]{2,1,0:T(8,128)(2,1)} %broadcast_in_dim.10), calls=%async_computation.1 | async-start | bytes 3145728 | tf_op jit(solution)/shard_map/all_to_all | solution.py:544
  138.7 6.3 %fusion.42 = (bf16[8,4,1,64,704]{4,3,2,1,0:T(8,128)(2,1)}, bf16[8,4,1,64,704]{4,3,2,1,0:T(8,128)(2,1)}) fusion(bf16[8,4,2,64,704]{4,3,2,1,0:T(8,128)(2,1)} %get-tuple-element.10), kind=kLoop, calls=%fused_computation.76 | loop fusion | bytes 11534336 | tf_op jit(solution)/shard_map/slice | solution.py:534
  144.9 14.3 %all-to-all-done.1 = bf16[8,48,2048]{2,1,0:T(8,128)(2,1)S(1)} async-done(((bf16[8,48,2048]{2,1,0:T(8,128)(2,1)}), bf16[8,48,2048]{2,1,0:T(8,128)(2,1)S(1)}, u32[]{:S(2)}, u32[]{:S(2)}) %all-to-all-start.1) | async-done | bytes 1572896 | tf_op jit(solution)/shard_map/all_to_all | solution.py:544
  159.3 3.6 %fusion.44 = f32[384,704]{0,1:T(8,128)S(1)} fusion(bf16[384,2048]{1,0:T(8,128)(2,1)S(1)} %bitcast.34, bf16[2048,704]{1,0:T(8,128)(2,1)} %bitcast.41), kind=kOutput, calls=%fused_computation.78 | convolution fusion | flops 1107296256 | bytes 5537792 | tf_op jit(solution)/shard_map/dot_general | solution.py:547
  162.9 7.0 %convolution_convert_fusion = bf16[384,2048]{1,0:T(8,128)(2,1)} fusion(bf16[2048,704]{1,0:T(8,128)(2,1)} %bitcast.32, bf16[384,2048]{1,0:T(8,128)(2,1)S(1)} %bitcast.35, bf16[2048,704]{1,0:T(8,128)(2,1)} %bitcast.31, f32[384,704]{0,1:T(8,128)S(1)} %fusion.44), kind=kOutput, calls=%fused_computation.1 | convolution fusion | flops 2217000960 | bytes 9994240 | tf_op jit(solution)/shard_map/dot_general | solution.py:550
  169.9 25.0 %all_to_all.29 = bf16[8,48,2048]{2,1,0:T(8,128)(2,1)S(1)} all-to-all(bf16[8,48,2048]{2,1,0:T(8,128)(2,1)} %bitcast.36), channel_id=1, replica_groups=mesh['z'=8,'y'=4,'x'=4,'c'=2] {'x','c'}, dimensions={0} | all-to-all | bytes 3145728 | tf_op jit(solution)/shard_map/all_to_all | solution.py:553
  194.9 0.2 convert_reduce_fusion
  195.1 0.3 fusion.40
  195.4 0.3 multiply_reduce_fusion
  195.7 0.9 multiply_convert_fusion
  (30 shorter events, 0.2 us)
Async XLA Ops:
  0.0 1.2 copy-start
  2.7 0.9 copy-start.1
  2.8 1.1 copy-start.7
  2.8 1.3 copy-start.5
  3.1 1.2 copy-start.8
  3.1 1.3 copy-start.3
  3.1 1.3 copy-start.4
  115.1 12.3 %all-to-all-start = ((bf16[8,48,256]{2,1,0:T(8,128)(2,1)}), bf16[8,48,256]{2,1,0:T(8,128)(2,1)S(1)}, u32[]{:S(2)}, u32[]{:S(2)}) async-start(bf16[8,48,256]{2,1,0:T(8,128)(2,1)} %bitcast.39), calls=%async_computation | async-start | bytes 393216 | tf_op jit(solution)/shard_map/all_to_all | solution.py:537
  127.4 5.3 %copy-start.2 = (f32[2048]{0:T(1024)S(1)}, f32[2048]{0:T(1024)}, u32[]{:S(2)}) copy-start(f32[2048]{0:T(1024)} %param.27) | copy-start | bytes 24580
  134.2 25.1 %all-to-all-start.1 = ((bf16[8,48,2048]{2,1,0:T(8,128)(2,1)}), bf16[8,48,2048]{2,1,0:T(8,128)(2,1)S(1)}, u32[]{:S(2)}, u32[]{:S(2)}) async-start(bf16[8,48,2048]{2,1,0:T(8,128)(2,1)} %broadcast_in_dim.10), calls=%async_computation.1 | async-start | bytes 3145728 | tf_op jit(solution)/shard_map/all_to_all | solution.py:544
  194.9 0.8 copy-start.6

commit v2 on v1

v2 whole, which is shorter than its diff:
```python
import functools
import math

import jax
import jax.numpy as jnp
from jax import lax
from jax.experimental import pallas as pl
from jax.experimental.pallas import tpu as pltpu
from jax.sharding import Mesh
from jax.sharding import PartitionSpec as P

NOPE = 128
RD = 64
VD = 128
NZ, NY, NX, NC = 8, 4, 4, 2
SP = ("z", "y")
TP = ("x", "c")
MESH = pl.DeviceIdType.MESH

eps_norm = 1e-05
rope_theta = 10000.0
resid_alpha = 8.0**0.25
HEADS_DEV = 2
WIDE = 384
QUART = 96
EXP2_SCALE = (NOPE + RD) ** (-0.5) * math.log2(math.e)
F32 = jnp.float32
BF16 = jnp.bfloat16


def rope_angles(positions):
    frequency = rope_theta ** (-jnp.arange(0, RD, 2, dtype=jnp.float32) / RD)
    angles = positions.astype(jnp.float32)[:, None] * frequency[None, :]
    return (jnp.cos(angles), jnp.sin(angles))


def rotate(values, cos_table, sin_table):
    half_width = values.shape[-1] // 2
    first_half = values[..., :half_width]
    second_half = values[..., half_width:]
    return jnp.concatenate(
        [
            first_half * cos_table - second_half * sin_table,
            second_half * cos_table + first_half * sin_table,
        ],
        axis=-1,
    )


def rms_scaled(latent, scaling):
    widened = latent.astype(jnp.float32)
    inverse = lax.rsqrt(jnp.mean(widened * widened, axis=-1, keepdims=True) + eps_norm)
    return (widened * inverse * scaling).astype(jnp.bfloat16)


def layer_scaled(stream, scaling):
    centre = stream - jnp.mean(stream, axis=-1, keepdims=True)
    spread = jnp.mean(centre * centre, axis=-1, keepdims=True)
    return centre * lax.rsqrt(spread + eps_norm) * scaling


class Wires:
    def __init__(self, targets):
        self.targets = targets
        self.sent = []

    def copy(self, src, dst, pair, index, way):
        send, recv = pair
        return pltpu.make_async_remote_copy(
            src_ref=src(),
            dst_ref=dst(),
            send_sem=send.at[index],
            recv_sem=recv.at[index],
            device_id=self.targets[way],
            device_id_type=MESH,
        )

    def start(self, src, dst, pair, index, way, size):
        self.copy(src, dst, pair, index, way).start()
        self.sent.append((src, dst, pair, index, way))

    def landed(self, slot, pair, index, way):
        self.copy(slot, slot, pair, index, way).wait_recv()

    def finish(self):
        for item in self.sent:
            self.copy(*item).wait_send()


class Ring:
    def __init__(self, wires, pair, block, me, at, part, chunk=None):
        self.w, self.pair, self.block = wires, pair, block
        self.at, self.part, self.chunk = at, part, chunk
        self.z, self.y = me
        self.yl, self.yr, self.yo = (self.y + 3) % 4, (self.y + 1) % 4, (self.y + 2) % 4
        self.zz = [(self.z + d) % 8 for d in range(8)]

    def send(self, slot, index, way, blocks):
        self.w.start(slot, slot, self.pair, index, way, blocks * self.block)

    def got(self, slot, index, way="y+"):
        self.w.landed(slot, self.pair, index, way)


class RingYZ(Ring):
    def y1(self):
        own = lambda: self.at(self.z, self.y)
        self.send(own, 0, "y+", 1)
        self.send(own, 1, "y-", 1)

    def y2(self):
        self.got(lambda: self.at(self.z, self.yl), 0)
        self.got(lambda: self.at(self.z, self.yr), 1)
        self.send(lambda: self.part(self.z, self.yl, 0), 2, "y+", 0.5)
        self.send(lambda: self.part(self.z, self.yr, 1), 3, "y-", 0.5)

    def z1(self):
        self.got(lambda: self.part(self.z, self.yo, 0), 2)
        self.got(lambda: self.part(self.z, self.yo, 1), 3)
        self.send(lambda: self.chunk(self.z, 0, 4), 4, "z+", 4)
        self.send(lambda: self.chunk(self.z, 0, 4), 8, "z-", 4)

    def zs(self, s):
        right, left = self.zz[9 - s], self.zz[s - 1]
        self.got(lambda: self.chunk(right, 0, 4), 4 + s - 2)
        self.got(lambda: self.chunk(left, 0, 4), 8 + s - 2)
        if s < 4:
            self.send(lambda: self.chunk(right, 0, 4), 4 + s - 1, "z+", 4)
            self.send(lambda: self.chunk(left, 0, 4), 8 + s - 1, "z-", 4)
        else:
            self.send(lambda: self.chunk(right, 0, 2), 7, "z+", 2)
            self.send(lambda: self.chunk(left, 2, 4), 11, "z-", 2)

    def z5(self):
        self.got(lambda: self.chunk(self.zz[4], 0, 2), 7)
        self.got(lambda: self.chunk(self.zz[4], 2, 4), 11)


class RingZY(Ring):
    def z1(self):
        own = lambda: self.at(self.z, self.y)
        self.send(own, 0, "z+", 1)
        self.send(own, 4, "z-", 1)

    def zs(self, s):
        right, left = self.zz[9 - s], self.zz[s - 1]
        self.got(lambda: self.at(right, self.y), s - 2)
        self.got(lambda: self.at(left, self.y), 4 + s - 2)
        if s < 4:
            self.send(lambda: self.at(right, self.y), s - 1, "z+", 1)
            self.send(lambda: self.at(left, self.y), 4 + s - 1, "z-", 1)
        else:
            self.send(lambda: self.part(right, self.y, 0), 3, "z+", 0.5)
            self.send(lambda: self.part(left, self.y, 1), 7, "z-", 0.5)

    def z5(self):
        self.got(lambda: self.part(self.zz[4], self.y, 0), 3)
        self.got(lambda: self.part(self.zz[4], self.y, 1), 7)

    def y1(self, *steps):
        for d in steps:
            zz = self.zz[d]
            self.send(lambda zz=zz: self.at(zz, self.y), 8 + 4 * d, "y+", 1)
            self.send(lambda zz=zz: self.at(zz, self.y), 9 + 4 * d, "y-", 1)

    def y2(self, *steps):
        for d in steps:
            zz = self.zz[d]
            self.got(lambda zz=zz: self.at(zz, self.yl), 8 + 4 * d)
            self.got(lambda zz=zz: self.at(zz, self.yr), 9 + 4 * d)
            self.send(lambda zz=zz: self.part(zz, self.yl, 0), 10 + 4 * d, "y+", 0.5)
            self.send(lambda zz=zz: self.part(zz, self.yr, 1), 11 + 4 * d, "y-", 0.5)

    def y3(self, *steps):
        for d in steps:
            zz = self.zz[d]
            self.got(lambda zz=zz: self.part(zz, self.yo, 0), 10 + 4 * d)
            self.got(lambda zz=zz: self.part(zz, self.yo, 1), 11 + 4 * d)


def plan(ka, kb, ga, gb, share, attend, stage):
    ka.y1()
    kb.z1()
    kb.y1(0)
    ka.y2()
    kb.zs(2)
    kb.y1(1, 7)
    ka.z1()
    share(0, 0)
    kb.y2(0)
    kb.zs(3)
    kb.y1(2, 6)
    kb.y3(0)
    share(1, 0)
    kb.y2(1, 7)

    def at_2():
        kb.zs(4)
        kb.y1(3, 5)
        ka.zs(2)
        share(0, 1, 7)
        kb.z5()
        kb.y1(4)
        kb.y3(1, 7)
        share(1, 1, 7)
        kb.y2(2, 6)
        ga.y1()
        gb.z1()

    def at_6():
        ka.zs(3)
        share(0, 2, 6)
        kb.y3(2, 6)
        share(1, 2, 6)
        kb.y2(3, 5)
        ga.y2()
        gb.zs(2)
        gb.y1(0)

    def at_10():
        ka.zs(4)
        share(0, 3, 5)
        kb.y3(3, 5)
        share(1, 3, 5)
        kb.y2(4)
        ga.z1()
        gb.zs(3)
        gb.y1(1, 7)

    def at_14():
        ka.z5()
        share(0, 4)
        kb.y3(4)
        share(1, 4)
        gb.y2(0)
        gb.zs(4)
        gb.y1(2, 6)

    attend({2: at_2, 6: at_6, 10: at_10, 14: at_14})
    stage("heads")
    gb.z5()
    gb.y1(3, 5)
    gb.y2(1, 7)
    gb.y3(0)
    ga.zs(2)
    stage("mix")
    gb.y1(4)
    gb.y2(2, 6)
    gb.y3(1, 7)
    stage("norm")
    ga.zs(3)
    gb.y2(3, 5)
    gb.y3(2, 6)
    stage("spread")
    gb.y2(4)
    ga.zs(4)
    stage("spread2")
    gb.y3(3, 5, 4)
    ga.z5()
    stage("ffn")


def layer_kernel(
    q_ref,
    kvm_ref,
    wg_ref,
    wu_ref,
    wd_ref,
    wkv_ref,
    wo_ref,
    res_ref,
    gain_ref,
    out_ref,
    kv,
    wa,
    wb,
    m_ref,
    l_ref,
    acc_ref,
    att,
    heads,
    wo,
    res,
    mid,
    normed,
    gate,
    up,
    part,
    pin,
    xin,
    loc_sem,
    ka_s,
    ka_r,
    kb_s,
    kb_r,
    kp_s,
    kp_r,
    wa_s,
    wa_r,
    wb_s,
    wb_r,
    hd_s,
    hd_r,
    nx_s,
    nx_r,
    pp_s,
    pp_r,
    px_s,
    px_r,
):
    z, y = lax.axis_index("z"), lax.axis_index("y")
    x, c = lax.axis_index("x"), lax.axis_index("c")
    other = 1 - c
    zz = [(z + d) % 8 for d in range(8)]
    xr, xl, xo = (x + 1) % 4, (x + 3) % 4, (x + 2) % 4

    own_rows = pl.multiple_of(c * 192, 96)
    res_rows = pl.multiple_of((x * 2 + c) * 48, 48)
    local = [
        pltpu.make_async_copy(kvm_ref.at[pl.ds(own_rows, 96)], kv.at[0, c, z, y], loc_sem.at[0]),
        pltpu.make_async_copy(
            kvm_ref.at[pl.ds(own_rows + 96, 96)], kv.at[1, c, z, y], loc_sem.at[1]
        ),
        pltpu.make_async_copy(wg_ref, wa.at[z, y], loc_sem.at[2]),
        pltpu.make_async_copy(wu_ref, wb.at[z, y, 0], loc_sem.at[3]),
        pltpu.make_async_copy(wd_ref, wb.at[z, y, 1], loc_sem.at[4]),
    ]
    later = [
        pltpu.make_async_copy(wo_ref, wo, loc_sem.at[5]),
        pltpu.make_async_copy(res_ref.at[pl.ds(res_rows, 48)], res, loc_sem.at[6]),
    ]
    for copy in local + later:
        copy.start()

    targets = {
        "z+": {"z": zz[1]},
        "z-": {"z": zz[7]},
        "y+": {"y": (y + 1) % 4},
        "y-": {"y": (y + 3) % 4},
        "c": {"c": other},
    }
    for dx in range(4):
        for dc in range(2):
            if dx or dc:
                targets[dx, dc] = {"x": (x + dx) % 4, "c": (c + dc) % 2}
    targets["x+"], targets["x-"] = targets[1, 0], targets[3, 0]
    barrier = pltpu.get_barrier_semaphore()
    greeted = ["z+", "z-", "y+", "y-"] + [k for k in targets if isinstance(k, tuple)]
    for way in greeted:
        pl.semaphore_signal(barrier, inc=1, device_id=targets[way], device_id_type=MESH)

    m_ref[...] = jnp.full(m_ref.shape, -1e30, F32)
    l_ref[...] = jnp.zeros(l_ref.shape, F32)
    acc_ref[...] = jnp.zeros(acc_ref.shape, F32)
    for copy in local:
        copy.wait()
    pl.semaphore_wait(barrier, len(greeted))

    wires = Wires(targets)
    me = (z, y)
    kv_bytes, w_bytes = QUART * WIDE * 2, 64 * 768 * 2
    ka = RingYZ(
        wires,
        (ka_s, ka_r),
        kv_bytes,
        me,
        lambda a, b: kv.at[0, c, a, b],
        lambda a, b, h: kv.at[0, c, a, b, pl.ds(48 * h, 48)],
        lambda a, lo, hi: kv.at[0, c, a, pl.ds(lo, hi - lo)],
    )
    kb = RingZY(
        wires,
        (kb_s, kb_r),
        kv_bytes,
        me,
        lambda a, b: kv.at[1, c, a, b],
        lambda a, b, h: kv.at[1, c, a, b, pl.ds(48 * h, 48)],
    )
    ga = RingYZ(
        wires,
        (wa_s, wa_r),
        w_bytes,
        me,
        lambda a, b: wa.at[a, b],
        lambda a, b, h: wa.at[a, b, pl.ds(32 * h, 32)],
        lambda a, lo, hi: wa.at[a, pl.ds(lo, hi - lo)],
    )
    gb = RingZY(
        wires,
        (wb_s, wb_r),
        2 * w_bytes,
        me,
        lambda a, b: wb.at[a, b],
        lambda a, b, h: wb.at[a, b, h],
    )

    def share(color, *steps):
        for d in steps:
            slot = lambda d=d: kv.at[color, c, zz[d]]
            wires.start(slot, slot, (kp_s, kp_r), 8 * color + d, "c", 4 * kv_bytes)

    def attend_unit(u):
        v = u + 2
        rnd, w = v // 4, v % 4
        color = w % 2
        d = jnp.where(w < 2, rnd, 8 - rnd) % 8
        at_z = (z + d) % 8
        wires.landed(lambda: kv.at[color, other, at_z], (kp_s, kp_r), 8 * color + d, "c")
        rows = kv[color, :, at_z].reshape(768, WIDE)
        extra = rows[:, 256:384]
        both = jnp.dot(rows[:, :256], wkv_ref[...], preferred_element_type=F32).astype(BF16)
        for h in range(HEADS_DEV):
            keys = jnp.concatenate([both[:, 128 * h : 128 * h + 128], extra], axis=1)
            vals = both[:, 256 + 128 * h : 384 + 128 * h]
            s = lax.dot_general(
                q_ref[h], keys, (((1,), (1,)), ((), ())), preferred_element_type=F32
            )
            top_old = m_ref[h]
            top = jnp.maximum(top_old, jnp.max(s, axis=1, keepdims=True))
            factor = jnp.exp2((top_old - top) * EXP2_SCALE)
            p = jnp.exp2((s - jnp.concatenate([top] * 6, axis=1)) * EXP2_SCALE)
            total = p[:, :128]
            for k in range(1, 6):
                total = total + p[:, 128 * k : 128 * k + 128]
            m_ref[h] = top
            l_ref[h] = l_ref[h] * factor + total
            acc_ref[h] = acc_ref[h] * factor + jnp.dot(
                p.astype(BF16), vals, preferred_element_type=F32
            )

    def attend(events):
        def step(u, carry):
            for k, event in events.items():
                pl.when(u == k)(event)
            attend_unit(u)
            return carry

        lax.fori_loop(0, 16, step, 0)

    heads_pair, norm_pair = (hd_s, hd_r), (nx_s, nx_r)
    core_pair, x_pair = (pp_s, pp_r), (px_s, px_r)
    cols = lambda h: pl.ds(1024 * h, 1024)

    def pass_on(slot, index):
        wires.start(slot, slot, norm_pair, index, "c", 0)

    def stage(name):
        if name == "heads":
            for h in range(HEADS_DEV):
                denom = jnp.sum(l_ref[h], axis=1, keepdims=True)
                done = (acc_ref[h] / denom).astype(BF16)
                att[:, :, 128 * h : 128 * h + 128] = done.reshape(8, 48, 128)
            for dx in range(4):
                for dc in range(2):
                    if dx or dc:
                        there = (x + dx) % 4 * 2 + (c + dc) % 2
                        wires.start(
                            lambda there=there: att.at[there],
                            lambda: heads.at[x * 2 + c],
                            heads_pair,
                            2 * dx + dc,
                            (dx, dc),
                            0,
                        )
            heads[x * 2 + c] = att[x * 2 + c]
        if name == "mix":
            for dx in range(4):
                for dc in range(2):
                    if dx or dc:
                        there = (x - dx + 4) % 4 * 2 + (c + dc) % 2
                        wires.landed(
                            lambda: heads.at[there], heads_pair, 2 * dx + dc, (dx, dc)
                        )
            for copy in later:
                copy.wait()
            rows = jnp.concatenate([heads[j] for j in range(8)], axis=1)

            def mix(n, carry):
                at = pl.ds(pl.multiple_of(n * 256, 256), 256)
                mid[:, at] = jnp.dot(rows, wo[:, at], preferred_element_type=F32)
                return carry

            lax.fori_loop(0, 8, mix, 0)
        if name == "norm":
            stream = resid_alpha * res[...].astype(F32) + mid[...]
            normed[x, c] = layer_scaled(stream, gain_ref[0:1, :]).astype(BF16)
            own = lambda: normed.at[x, c]
            wires.start(own, own, norm_pair, 0, "x+", 0)
            wires.start(own, own, norm_pair, 1, "x-", 0)
            pass_on(own, 4)
        if name == "spread":
            wires.landed(lambda: normed.at[xl, c], norm_pair, 0, "x+")
            wires.landed(lambda: normed.at[xr, c], norm_pair, 1, "x-")
            slot = lambda: normed.at[xl, c, :, cols(0)]
            wires.start(slot, slot, norm_pair, 2, "x+", 0)
            slot_r = lambda: normed.at[xr, c, :, cols(1)]
            wires.start(slot_r, slot_r, norm_pair, 3, "x-", 0)
            pass_on(lambda: normed.at[xl, c], 5)
            pass_on(lambda: normed.at[xr, c], 6)
        if name == "spread2":
            wires.landed(lambda: normed.at[xo, c, :, cols(0)], norm_pair, 2, "x+")
            wires.landed(lambda: normed.at[xo, c, :, cols(1)], norm_pair, 3, "x-")
            pass_on(lambda: normed.at[xo, c], 7)
            for index, at in ((4, x), (5, xl), (6, xr), (7, xo)):
                wires.landed(lambda: normed.at[at, other], norm_pair, index, "c")
        if name == "ffn":
            for k in range(4):
                rows = normed[:, :, :, 512 * k : 512 * k + 512].reshape(384, 512)
                for w, total in (
                    (wa[2 * k : 2 * k + 2].reshape(512, 704), gate),
                    (wb[2 * k : 2 * k + 2, :, 0].reshape(512, 704), up),
                ):
                    term = jnp.dot(rows, w, preferred_element_type=F32)
                    total[...] = term if k == 0 else total[...] + term
            v = gate[...]
            hidden = (v / (1.0 + jnp.exp(-v)) * up[...]).astype(BF16)
            for k in range(8):
                w = wb[k, :, 1].reshape(256, 704)
                term = lax.dot_general(
                    hidden, w, (((1,), (1,)), ((), ())), preferred_element_type=F32
                )
                at = pl.ds(256 * k, 256)
                part[:, :, :, at] = term.astype(BF16).reshape(4, 2, 48, 256)
                wires.start(
                    lambda at=at: part.at[:, other, :, at],
                    lambda at=at: pin.at[:, :, at],
                    core_pair,
                    k,
                    "c",
                    0,
                )
            for k in range(8):
                wires.landed(lambda: pin.at[:, :, pl.ds(256 * k, 256)], core_pair, k, "c")

            def pair_sum(at_x, lo, hi):
                return part[at_x, c, :, lo:hi].astype(F32) + pin[at_x, :, lo:hi].astype(F32)

            def x_send(index, at_x, h, way):
                wires.start(
                    lambda: pin.at[at_x, :, cols(h)], lambda: xin.at[index], x_pair, index, way, 0
                )

            for at_x, h in ((xo, 0), (xo, 1), (xr, 1), (xl, 0)):
                half = slice(1024 * h, 1024 * h + 1024)
                pin[at_x, :, half] = pair_sum(at_x, half.start, half.stop).astype(BF16)
            x_send(0, xo, 0, "x+")
            x_send(1, xo, 1, "x-")
            x_send(2, xr, 1, "x+")
            x_send(3, xl, 0, "x-")
            near_r = pair_sum(xr, 0, 1024)
            near_l = pair_sum(xl, 1024, 2048)
            wires.landed(lambda: xin.at[0], x_pair, 0, "x+")
            pin[xr, :, 0:1024] = (near_r + xin[0].astype(F32)).astype(BF16)
            x_send(4, xr, 0, "x+")
            wires.landed(lambda: xin.at[1], x_pair, 1, "x-")
            pin[xl, :, 1024:2048] = (near_l + xin[1].astype(F32)).astype(BF16)
            x_send(5, xl, 1, "x-")
            for index, way in ((2, "x+"), (3, "x-"), (4, "x+"), (5, "x-")):
                wires.landed(lambda: xin.at[index], x_pair, index, way)
            low = pair_sum(x, 0, 1024) + xin[4].astype(F32) + xin[3].astype(F32)
            high = pair_sum(x, 1024, 2048) + xin[2].astype(F32) + xin[5].astype(F32)
            ffn_sum = jnp.concatenate([low, high], axis=1)
            stream = resid_alpha * normed[x, c].astype(F32) + 0.5 * ffn_sum
            out_ref[...] = layer_scaled(stream, gain_ref[1:2, :]).astype(BF16)

    plan(ka, kb, ga, gb, share, attend, stage)
    wires.finish()


def body(
    resid_stream,
    q_latent,
    kv_latent,
    rope_key,
    doc_ids,
    q_gain,
    kv_gain,
    w_query,
    w_key,
    w_value,
    w_out,
    mix_gain,
    w_gate,
    w_up,
    w_down,
    out_gain,
):
    tok_rows = q_latent.shape[0]
    positions = lax.axis_index(SP) * tok_rows + jnp.arange(tok_rows, dtype=jnp.int32)
    cos_table, sin_table = rope_angles(positions)
    q_normed = rms_scaled(q_latent, q_gain)
    queries = jnp.dot(q_normed, w_query, preferred_element_type=jnp.float32).reshape(
        tok_rows, HEADS_DEV, NOPE + RD
    )
    kv_normed = rms_scaled(kv_latent, kv_gain)
    key_rot = rotate(rope_key.astype(jnp.float32), cos_table, sin_table).astype(jnp.bfloat16)
    slots = jnp.arange(64, dtype=jnp.int32)
    same = doc_ids[:, None] == slots[None, :]
    message = jnp.concatenate([kv_normed, key_rot, same.astype(BF16)], axis=1)
    apart = jnp.where(same | (slots >= 4)[None, :], 0.0, -1e30).astype(BF16)
    q_heads = []
    for h in range(HEADS_DEV):
        q_heads.append(
            jnp.concatenate(
                [
                    queries[:, h, :NOPE].astype(BF16),
                    rotate(queries[:, h, NOPE:], cos_table, sin_table).astype(BF16),
                    apart,
                ],
                axis=1,
            )
        )
    q_all = jnp.stack(q_heads)
    wkv = jnp.concatenate([w_key, w_value], axis=1)

    any_spec = pl.BlockSpec(memory_space=pl.ANY)
    vmem_spec = pl.BlockSpec(memory_space=pltpu.VMEM)
    dma = pltpu.SemaphoreType.DMA
    vmem = pltpu.VMEM
    sizes = (12, 40, 16, 12, 40, 8, 8, 8, 6)
    return pl.pallas_call(
        layer_kernel,
        out_shape=jax.ShapeDtypeStruct((48, 2048), BF16),
        in_specs=[vmem_spec] + [any_spec] * 4 + [vmem_spec] + [any_spec] * 2 + [vmem_spec],
        out_specs=vmem_spec,
        scratch_shapes=[
            vmem((2, NC, NZ, NY, QUART, WIDE), BF16),
            vmem((NZ, NY, 64, 704), BF16),
            vmem((NZ, NY, 2, 64, 704), BF16),
            vmem((HEADS_DEV, tok_rows, 128), F32),
            vmem((HEADS_DEV, tok_rows, 128), F32),
            vmem((HEADS_DEV, tok_rows, 128), F32),
            vmem((8, 48, 256), BF16),
            vmem((8, 48, 256), BF16),
            vmem((2048, 2048), BF16),
            vmem((48, 2048), BF16),
            vmem((48, 2048), F32),
            vmem((NX, NC, 48, 2048), BF16),
            vmem((tok_rows, 704), F32),
            vmem((tok_rows, 704), F32),
            vmem((NX, NC, 48, 2048), BF16),
            vmem((NX, 48, 2048), BF16),
            vmem((6, 48, 1024), BF16),
            dma((8,)),
        ]
        + [dma((n,)) for n in sizes for _ in range(2)],
        compiler_params=pltpu.CompilerParams(
            collective_id=0, has_side_effects=True, vmem_limit_bytes=60 * 1024 * 1024
        ),
        name="whole_layer",
    )(
        q_all,
        message,
        w_gate,
        w_up,
        w_down.T,
        wkv,
        w_out,
        resid_stream,
        jnp.stack([mix_gain, out_gain]),
    )


def solution(mesh):
    split = Mesh(mesh.devices.reshape(NZ, NY, NX, NC), ("z", "y", "x", "c"))
    in_specs = (
        P(SP, None),
        P(SP, None),
        P(SP, None),
        P(SP, None),
        P(SP),
        P(),
        P(),
        P(None, TP),
        P(None, TP),
        P(None, TP),
        P(),
        P(),
        P(SP, TP),
        P(SP, TP),
        P(TP, SP),
        P(),
    )
    out_specs = P((*SP, *TP), None)
    return jax.shard_map(body, mesh=split, in_specs=in_specs, out_specs=out_specs, check_vma=False)
```

time: 197 us -> 135 us (0.69)
  blocking collectives: 25 us -> 0 us
  waiting for transfers between devices: 20.2 us -> 0 us
  Pallas kernels: 107 us -> 124 us
  matrix products: 17.2 us -> 1.5 us
  starting transfers between devices: 10.9 us -> 0 us
  local copies, waits for them, and re-layouts: 8.6 us -> 2.87 us
    all_to_all x1 -> x0, blocking collectives: 25 us -> none  [body(): lax.all_to_all(down_term.astype(BF16).reshape(8, part_rows, 2048), TP, 0,...]
    all_to_all x2 -> x0, waiting for transfers between devices: 20.2 us -> none  [the longest x1 14.3 us: body(): lax.all_to_all(copies, TP, split_axis=0, concat_axis=0, tiled=True)]
    pallas_call x1, Pallas kernels: 107 us -> 124 us  [body(): pl.pallas_call(layer_kernel, out_shape=jax.ShapeDtypeStruct((48, 2048), B...]
    dot_general x3 -> x0, matrix products: 15.7 us -> none  [the longest x1 7.04 us: body(): lax.dot_general(hidden, wd_all, (((1,), (1,)), ((), ())), preferred_eleme...]
    all_to_all x2 -> x0, starting transfers between devices: 10.9 us -> none  [the longest x1 6.43 us: body(): lax.all_to_all(attended, TP, split_axis=0, concat_axis=1, tiled=True)]
    slice x1 -> x0, local copies, waits for them, and re-layouts: 6.29 us -> none  [body(): wu_all = wb[:, :, 0].reshape(2048, 704)]
  transfers between devices with their start and end apart: 2 -> 0, of which waited for: 2 -> 0; matrix products, arithmetic and copies ran while one was open for 3% -> 0% of each run, Pallas kernels for 0% -> 0%
where the time goes in v2:
time: 135 us
  Pallas kernels  124 us (92%)
  other arithmetic  6.57 us (5%)
  local copies, waits for them, and re-layouts  2.87 us (2%)
  matrix products  1.5 us (1%)
    pallas_call x1, Pallas kernels, body(): pl.pallas_call(layer_kernel, out_shape=jax.ShapeDtypeStruct((48, 2048), B...  124 us

profile of v2, /device:TPU:1, one launch (start us, length us, event | category | flops | bytes accessed | tf_op | source)
XLA Modules:
  0.0 135.1 jit_solution(17000415923477519827)
XLA Ops:
  0.0 0.0 copy-start
  0.0 0.0 copy-start.4
  0.0 0.0 copy-start.1
  0.0 0.0 copy-start.7
  0.0 0.0 copy-start.3
  0.0 0.0 copy-start.2
  0.0 0.0 copy-start.6
  0.1 0.0 copy-start.5
  0.1 1.2 fusion
  1.3 0.0 copy-done
  1.3 1.5 %fusion.6 = f32[384,384]{0,1:T(8,128)S(1)} fusion(bf16[512,384]{1,0:T(8,128)(2,1)S(1)} %copy-done, bf16[384,512]{1,0:T(8,128)(2,1)} %param.17, f32[512]{0:T(512)} %param.21, f32[384]{0:T(512)S(1)} %add_rsqrt_fusion.1), kind=kOutput, calls=%fused_computation.10 | convolution fusion | flops 151781376 | bytes 1379840 | tf_op jit(solution)/shard_map/dot_general | solution.py:592
  2.8 0.3 copy.22
  3.1 0.9 copy.26
  4.1 0.9 fusion.33
  5.1 0.8 select_convert_fusion
  5.9 0.2 fusion.22
  6.1 0.8 pad_maximum_fusion.q_ref
  6.9 0.0 copy-done.1
  6.9 0.1 fusion.3
  7.0 0.0 copy-done.7
  7.0 0.1 fusion.5
  7.2 0.0 copy-done.4
  7.2 0.1 fusion.36
  7.3 0.8 pad_maximum_fusion.1.kvm_ref
  8.1 0.0 copy-done.3
  8.1 0.0 copy-done.2
  8.2 0.7 pad_maximum_fusion.2.wkv_ref
  8.9 0.0 copy-done.6
  8.9 0.0 copy-done.5
  8.9 0.6 pad_maximum_fusion.5.gain_ref
  9.5 124.0 %whole_layer.1 = bf16[48,2048]{1,0:T(8,128)(2,1)} custom-call(bf16[2,384,256]{2,1,0:T(8,128)(2,1)} %pad_maximum_fusion.q_ref, bf16[384,384]{1,0:T(8,128)(2,1)} %pad_maximum_fusion.1.kvm_ref, bf16[64,704]{1,0:T(8,128)(2,1)} %wg_ref.1, bf16[64,704]{1,0:T(8,128)(2,1)} %wu_ref.1, bf16[64,704]{1,0:T(8,128)(2,1)} %bitcast.18, ...), custom_call_target="tpu_custom_call" | custom-call | tf_op jit(solution)/shard_map/whole_layer/pallas_call | solution.py:621
  133.5 1.6 %copy.28 = bf16[48,2048]{1,0:T(8,128)(2,1)} copy(bf16[48,2048]{1,0:T(8,128)(2,1)} %whole_layer.1) | data formatting | bytes 393216
  (9 shorter events, 0.1 us)
Async XLA Ops:
  0.0 1.3 copy-start
  0.0 7.2 %copy-start.4 = (s32[384]{0:T(512)S(1)}, s32[384]{0:T(512)}, u32[]{:S(2)}) copy-start(s32[384]{0:T(512)} %param.20) | copy-start | bytes 4612
  0.0 6.9 %copy-start.1 = (bf16[384,256]{1,0:T(8,128)(2,1)S(1)}, bf16[384,256]{1,0:T(8,128)(2,1)}, u32[]{:S(2)}) copy-start(bf16[384,256]{1,0:T(8,128)(2,1)} %param.18) | copy-start | bytes 589828
  0.0 7.0 %copy-start.7 = (f32[256]{0:T(256)S(1)}, f32[256]{0:T(256)}, u32[]{:S(2)}) copy-start(f32[256]{0:T(256)} %param.22) | copy-start | bytes 3076
  0.0 8.1 %copy-start.3 = (bf16[256,256]{1,0:T(8,128)(2,1)S(1)}, bf16[256,256]{1,0:T(8,128)(2,1)}, u32[]{:S(2)}) copy-start(bf16[256,256]{1,0:T(8,128)(2,1)} %param.24) | copy-start | bytes 393220
  0.0 8.1 %copy-start.2 = (bf16[256,256]{1,0:T(8,128)(2,1)S(1)}, bf16[256,256]{1,0:T(8,128)(2,1)}, u32[]{:S(2)}) copy-start(bf16[256,256]{1,0:T(8,128)(2,1)} %param.25) | copy-start | bytes 393220
  0.0 8.8 %copy-start.6 = (f32[2048]{0:T(1024)S(1)}, f32[2048]{0:T(1024)}, u32[]{:S(2)}) copy-start(f32[2048]{0:T(1024)} %param.27) | copy-start | bytes 24580
  0.1 8.8 %copy-start.5 = (f32[2048]{0:T(1024)S(1)}, f32[2048]{0:T(1024)}, u32[]{:S(2)}) copy-start(f32[2048]{0:T(1024)} %param.31) | copy-start | bytes 24580

commit v3 on v2

--- a/solution.py
+++ b/solution.py
@@ -22,7 +22,7 @@
 resid_alpha = 8.0**0.25
 HEADS_DEV = 2
 WIDE = 384
-QUART = 96
+A_ROWS, B_ROWS = 64, 32
 EXP2_SCALE = (NOPE + RD) ** (-0.5) * math.log2(math.e)
 F32 = jnp.float32
 BF16 = jnp.bfloat16
@@ -178,85 +178,154 @@
             self.got(lambda zz=zz: self.part(zz, self.yo, 1), 11 + 4 * d)
 
 
-def plan(ka, kb, ga, gb, share, attend, stage):
+def plan(ka, kb, ga, gb, across, across2, attend, stage):
     ka.y1()
+    kb.y1(0)
     kb.z1()
-    kb.y1(0)
-    ka.y2()
+    gb.z1()
+    gb.y1(0)
     kb.zs(2)
     kb.y1(1, 7)
-    ka.z1()
-    share(0, 0)
+    ka.y2()
     kb.y2(0)
+    ga.y1()
+    gb.zs(2)
     kb.zs(3)
     kb.y1(2, 6)
+    kb.y2(1, 7)
+    ka.z1()
+    across(0, 0)
     kb.y3(0)
-    share(1, 0)
-    kb.y2(1, 7)
-
-    def at_2():
-        kb.zs(4)
-        kb.y1(3, 5)
+    across(1, 0)
+    gb.y1(1)
+    kb.y2(2, 6)
+    kb.y3(1)
+    across(1, 1)
+    kb.y3(7)
+    across(1, 7)
+    across2(0, 0)
+    kb.zs(4)
+    kb.y1(3, 5)
+    across2(1, 0)
+    gb.zs(3)
+
+    def at_0_1():
+        across2(1, 1, 7)
+        gb.y1(2)
+
+    def at_1_0():
         ka.zs(2)
-        share(0, 1, 7)
+        across(0, 1, 7)
+        kb.y3(6)
+        across(1, 6)
+        kb.y2(3)
         kb.z5()
         kb.y1(4)
-        kb.y3(1, 7)
-        share(1, 1, 7)
-        kb.y2(2, 6)
-        ga.y1()
-        gb.z1()
-
-    def at_6():
+        kb.y2(5)
+        kb.y3(2)
+        across(1, 2)
+        gb.y2(1)
+        across2(0, 1)
+        gb.zs(4)
+        gb.y1(5)
+        kb.y3(3)
+        across(1, 3)
+        kb.y2(4)
+
+    def at_1_1():
+        across2(0, 7)
+        kb.y3(5)
+        across(1, 5)
+
+    def at_2_0():
+        across2(1, 6, 2)
         ka.zs(3)
-        share(0, 2, 6)
-        kb.y3(2, 6)
-        share(1, 2, 6)
-        kb.y2(3, 5)
+        across(0, 2, 6)
+        gb.y3(1)
+
+    def at_2_1():
+        across2(1, 3)
+        gb.z5()
+        gb.y1(4)
+
+    def at_3_0():
+        across2(1, 5)
+        kb.y3(4)
+        across(1, 4)
+        across2(0, 2)
         ga.y2()
-        gb.zs(2)
-        gb.y1(0)
-
-    def at_10():
+
+    def at_3_1():
         ka.zs(4)
-        share(0, 3, 5)
-        kb.y3(3, 5)
-        share(1, 3, 5)
-        kb.y2(4)
+        across(0, 3, 5)
+        across2(0, 6)
+        gb.y2(5)
+
+    def at_4_0():
+        across2(1, 4)
+        gb.y1(3)
         ga.z1()
-        gb.zs(3)
-        gb.y1(1, 7)
-
-    def at_14():
+
+    def at_5_0():
         ka.z5()
-        share(0, 4)
-        kb.y3(4)
-        share(1, 4)
-        gb.y2(0)
-        gb.zs(4)
-        gb.y1(2, 6)
-
-    attend({2: at_2, 6: at_6, 10: at_10, 14: at_14})
+        across(0, 4)
+        across2(0, 3)
+        gb.y3(5)
+        gb.y2(2)
+        across2(0, 5)
+
+    def at_5_1():
+        gb.y2(4)
+
+    def at_6_0():
+        across2(0, 4)
+        gb.y1(7)
+
+    def at_6_1():
+        gb.y3(2)
+
+    def at_7_0():
+        ga.zs(2)
+        gb.y3(4)
+
+    def at_7_1():
+        gb.y1(6)
+
+    attend(
+        {
+            (0, 1): at_0_1,
+            (1, 0): at_1_0,
+            (1, 1): at_1_1,
+            (2, 0): at_2_0,
+            (2, 1): at_2_1,
+            (3, 0): at_3_0,
+            (3, 1): at_3_1,
+            (4, 0): at_4_0,
+            (5, 0): at_5_0,
+            (5, 1): at_5_1,
+            (6, 0): at_6_0,
+            (6, 1): at_6_1,
+            (7, 0): at_7_0,
+            (7, 1): at_7_1,
+        }
+    )
     stage("heads")
-    gb.z5()
-    gb.y1(3, 5)
-    gb.y2(1, 7)
-    gb.y3(0)
-    ga.zs(2)
+    gb.y2(7, 0)
     stage("mix")
-    gb.y1(4)
-    gb.y2(2, 6)
-    gb.y3(1, 7)
+    gb.y2(6)
+    ga.zs(3)
+    gb.y3(7)
     stage("norm")
-    ga.zs(3)
-    gb.y2(3, 5)
-    gb.y3(2, 6)
+    gb.y2(3)
+    gb.y3(0, 6, 3)
     stage("spread")
-    gb.y2(4)
     ga.zs(4)
     stage("spread2")
-    gb.y3(3, 5, 4)
+    stage("gate0")
+    stage("gate1")
+    stage("gate2")
     ga.z5()
+    stage("gate3")
     stage("ffn")
 
 
@@ -271,7 +340,8 @@
     res_ref,
     gain_ref,
     out_ref,
-    kv,
+    kva,
+    kvb,
     wa,
     wb,
     m_ref,
@@ -295,6 +365,8 @@
     kb_r,
     kp_s,
     kp_r,
+    kx_s,
+    kx_r,
     wa_s,
     wa_r,
     wb_s,
@@ -314,12 +386,16 @@
     zz = [(z + d) % 8 for d in range(8)]
     xr, xl, xo = (x + 1) % 4, (x + 3) % 4, (x + 2) % 4
 
-    own_rows = pl.multiple_of(c * 192, 96)
+    par = x % 2
+    apar = 1 - par
+    own_rows = pl.multiple_of(c * 192 + par * 96, 32)
     res_rows = pl.multiple_of((x * 2 + c) * 48, 48)
     local = [
-        pltpu.make_async_copy(kvm_ref.at[pl.ds(own_rows, 96)], kv.at[0, c, z, y], loc_sem.at[0]),
         pltpu.make_async_copy(
-            kvm_ref.at[pl.ds(own_rows + 96, 96)], kv.at[1, c, z, y], loc_sem.at[1]
+            kvm_ref.at[pl.ds(own_rows, A_ROWS)], kva.at[par, c, z, y], loc_sem.at[0]
+        ),
+        pltpu.make_async_copy(
+            kvm_ref.at[pl.ds(own_rows + A_ROWS, B_ROWS)], kvb.at[par, c, z, y], loc_sem.at[1]
         ),
         pltpu.make_async_copy(wg_ref, wa.at[z, y], loc_sem.at[2]),
         pltpu.make_async_copy(wu_ref, wb.at[z, y, 0], loc_sem.at[3]),
@@ -358,23 +434,23 @@
 
     wires = Wires(targets)
     me = (z, y)
-    kv_bytes, w_bytes = QUART * WIDE * 2, 64 * 768 * 2
+    row_bytes, w_bytes = WIDE * 2, 64 * 768 * 2
     ka = RingYZ(
         wires,
         (ka_s, ka_r),
-        kv_bytes,
+        A_ROWS * row_bytes,
         me,
-        lambda a, b: kv.at[0, c, a, b],
-        lambda a, b, h: kv.at[0, c, a, b, pl.ds(48 * h, 48)],
-        lambda a, lo, hi: kv.at[0, c, a, pl.ds(lo, hi - lo)],
+        lambda a, b: kva.at[par, c, a, b],
+        lambda a, b, h: kva.at[par, c, a, b, pl.ds(32 * h, 32)],
+        lambda a, lo, hi: kva.at[par, c, a, pl.ds(lo, hi - lo)],
     )
     kb = RingZY(
         wires,
         (kb_s, kb_r),
-        kv_bytes,
+        B_ROWS * row_bytes,
         me,
-        lambda a, b: kv.at[1, c, a, b],
-        lambda a, b, h: kv.at[1, c, a, b, pl.ds(48 * h, 48)],
+        lambda a, b: kvb.at[par, c, a, b],
+        lambda a, b, h: kvb.at[par, c, a, b, pl.ds(16 * h, 16)],
     )
     ga = RingYZ(
         wires,
@@ -394,48 +470,72 @@
         lambda a, b, h: wb.at[a, b, h],
     )
 
-    def share(color, *steps):
+    keys_of = (kva, kvb)
+
+    def pair_with(color, d, theirs):
+        own = apar if theirs else par
+        slot = lambda: keys_of[color].at[own, c, zz[d]]
+        wires.start(slot, slot, (kp_s, kp_r), 16 * theirs + 8 * color + d, "c", 0)
+
+    def across(color, *steps):
         for d in steps:
-            slot = lambda d=d: kv.at[color, c, zz[d]]
-            wires.start(slot, slot, (kp_s, kp_r), 8 * color + d, "c", 4 * kv_bytes)
-
-    def attend_unit(u):
-        v = u + 2
-        rnd, w = v // 4, v % 4
-        color = w % 2
-        d = jnp.where(w < 2, rnd, 8 - rnd) % 8
+            for h, way in ((0, "x+"), (1, "x-")):
+                slot = lambda d=d, h=h: keys_of[color].at[par, c, zz[d], pl.ds(2 * h, 2)]
+                wires.start(slot, slot, (kx_s, kx_r), 16 * h + 8 * color + d, way, 0)
+            pair_with(color, d, 0)
+
+    def across2(color, *steps):
+        for d in steps:
+            for h, way in ((0, "x+"), (1, "x-")):
+                slot = lambda: keys_of[color].at[apar, c, zz[d], pl.ds(2 * h, 2)]
+                wires.landed(slot, (kx_s, kx_r), 16 * h + 8 * color + d, way)
+            pair_with(color, d, 1)
+
+    def attend_unit(u, h):
+        d = jnp.where(u % 2 == 1, (u + 1) // 2, (8 - u // 2) % 8)
         at_z = (z + d) % 8
-        wires.landed(lambda: kv.at[color, other, at_z], (kp_s, kp_r), 8 * color + d, "c")
-        rows = kv[color, :, at_z].reshape(768, WIDE)
+        if h == 0:
+            for theirs, own in ((0, par), (1, apar)):
+                for color, keys in enumerate(keys_of):
+                    wires.landed(
+                        lambda: keys.at[own, other, at_z],
+                        (kp_s, kp_r),
+                        16 * theirs + 8 * color + d,
+                        "c",
+                    )
+        rows = jnp.concatenate(
+            [kva[:, :, at_z].reshape(1024, WIDE), kvb[:, :, at_z].reshape(512, WIDE)], axis=0
+        )
         extra = rows[:, 256:384]
-        both = jnp.dot(rows[:, :256], wkv_ref[...], preferred_element_type=F32).astype(BF16)
-        for h in range(HEADS_DEV):
-            keys = jnp.concatenate([both[:, 128 * h : 128 * h + 128], extra], axis=1)
-            vals = both[:, 256 + 128 * h : 384 + 128 * h]
-            s = lax.dot_general(
-                q_ref[h], keys, (((1,), (1,)), ((), ())), preferred_element_type=F32
-            )
-            top_old = m_ref[h]
-            top = jnp.maximum(top_old, jnp.max(s, axis=1, keepdims=True))
-            factor = jnp.exp2((top_old - top) * EXP2_SCALE)
-            p = jnp.exp2((s - jnp.concatenate([top] * 6, axis=1)) * EXP2_SCALE)
-            total = p[:, :128]
-            for k in range(1, 6):
-                total = total + p[:, 128 * k : 128 * k + 128]
-            m_ref[h] = top
-            l_ref[h] = l_ref[h] * factor + total
-            acc_ref[h] = acc_ref[h] * factor + jnp.dot(
-                p.astype(BF16), vals, preferred_element_type=F32
-            )
+        both = jnp.dot(rows[:, :256], wkv_ref[h], preferred_element_type=F32).astype(BF16)
+        keys = jnp.concatenate([both[:, :128], extra], axis=1)
+        vals = both[:, 128:]
+        s = lax.dot_general(
+            q_ref[h], keys, (((1,), (1,)), ((), ())), preferred_element_type=F32
+        )
+        top_old = m_ref[h]
+        top = jnp.maximum(top_old, jnp.max(s, axis=1, keepdims=True))
+        factor = jnp.exp2((top_old - top) * EXP2_SCALE)
+        p = jnp.exp2((s - jnp.concatenate([top] * 12, axis=1)) * EXP2_SCALE)
+        total = p[:, :128]
+        for k in range(1, 12):
+            total = total + p[:, 128 * k : 128 * k + 128]
+        m_ref[h] = top
+        l_ref[h] = l_ref[h] * factor + total
+        acc_ref[h] = acc_ref[h] * factor + jnp.dot(
+            p.astype(BF16), vals, preferred_element_type=F32
+        )
 
     def attend(events):
         def step(u, carry):
-            for k, event in events.items():
-                pl.when(u == k)(event)
-            attend_unit(u)
+            for h in range(HEADS_DEV):
+                for (k, at_h), event in events.items():
+                    if at_h == h:
+                        pl.when(u == k)(event)
+                attend_unit(u, h)
             return carry
 
-        lax.fori_loop(0, 16, step, 0)
+        lax.fori_loop(0, 8, step, 0)
 
     heads_pair, norm_pair = (hd_s, hd_r), (nx_s, nx_r)
     core_pair, x_pair = (pp_s, pp_r), (px_s, px_r)
@@ -503,15 +603,26 @@
             pass_on(lambda: normed.at[xo, c], 7)
             for index, at in ((4, x), (5, xl), (6, xr), (7, xo)):
                 wires.landed(lambda: normed.at[at, other], norm_pair, index, "c")
+        if name[:4] == "gate":
+            k = int(name[4:])
+            near, far = ((0, 1), (7, 2), (6, 3), (5, 4))[k]
+            at = [zz[near], zz[far]]
+            rows = jnp.concatenate(
+                [
+                    normed[:, :, :, pl.ds(pl.multiple_of(256 * a, 256), 256)].reshape(384, 256)
+                    for a in at
+                ],
+                axis=1,
+            )
+            for weight, total in (
+                ([wa[a].reshape(256, 704) for a in at], gate),
+                ([wb[a, :, 0].reshape(256, 704) for a in at], up),
+            ):
+                term = jnp.dot(
+                    rows, jnp.concatenate(weight, axis=0), preferred_element_type=F32
+                )
+                total[...] = term if k == 0 else total[...] + term
         if name == "ffn":
-            for k in range(4):
-                rows = normed[:, :, :, 512 * k : 512 * k + 512].reshape(384, 512)
-                for w, total in (
-                    (wa[2 * k : 2 * k + 2].reshape(512, 704), gate),
-                    (wb[2 * k : 2 * k + 2, :, 0].reshape(512, 704), up),
-                ):
-                    term = jnp.dot(rows, w, preferred_element_type=F32)
-                    total[...] = term if k == 0 else total[...] + term
             v = gate[...]
             hidden = (v / (1.0 + jnp.exp(-v)) * up[...]).astype(BF16)
             for k in range(8):
@@ -563,7 +674,7 @@
             stream = resid_alpha * normed[x, c].astype(F32) + 0.5 * ffn_sum
             out_ref[...] = layer_scaled(stream, gain_ref[1:2, :]).astype(BF16)
 
-    plan(ka, kb, ga, gb, share, attend, stage)
+    plan(ka, kb, ga, gb, across, across2, attend, stage)
     wires.finish()
 
 
@@ -611,20 +722,26 @@
             )
         )
     q_all = jnp.stack(q_heads)
-    wkv = jnp.concatenate([w_key, w_value], axis=1)
+    wkv = jnp.stack(
+        [
+            jnp.concatenate([w[:, 128 * h : 128 * h + 128] for w in (w_key, w_value)], axis=1)
+            for h in range(HEADS_DEV)
+        ]
+    )
 
     any_spec = pl.BlockSpec(memory_space=pl.ANY)
     vmem_spec = pl.BlockSpec(memory_space=pltpu.VMEM)
     dma = pltpu.SemaphoreType.DMA
     vmem = pltpu.VMEM
-    sizes = (12, 40, 16, 12, 40, 8, 8, 8, 6)
+    sizes = (12, 40, 32, 32, 12, 40, 8, 8, 8, 6)
     return pl.pallas_call(
         layer_kernel,
         out_shape=jax.ShapeDtypeStruct((48, 2048), BF16),
         in_specs=[vmem_spec] + [any_spec] * 4 + [vmem_spec] + [any_spec] * 2 + [vmem_spec],
         out_specs=vmem_spec,
         scratch_shapes=[
-            vmem((2, NC, NZ, NY, QUART, WIDE), BF16),
+            vmem((2, NC, NZ, NY, A_ROWS, WIDE), BF16),
+            vmem((2, NC, NZ, NY, B_ROWS, WIDE), BF16),
             vmem((NZ, NY, 64, 704), BF16),
             vmem((NZ, NY, 2, 64, 704), BF16),
             vmem((HEADS_DEV, tok_rows, 128), F32),

time: 135 us -> 118 us (0.87)
  Pallas kernels: 124 us -> 106 us
    pallas_call x1, Pallas kernels: 124 us -> 106 us  [body(): pl.pallas_call(layer_kernel, out_shape=jax.ShapeDtypeStruct((48, 2048), B...]
where the time goes in v3:
time: 118 us
  Pallas kernels  106 us (90%)
  other arithmetic  6.58 us (6%)
  local copies, waits for them, and re-layouts  2.89 us (2%)
  matrix products  1.5 us (1%)
    pallas_call x1, Pallas kernels, body(): pl.pallas_call(layer_kernel, out_shape=jax.ShapeDtypeStruct((48, 2048), B...  106 us
    unnamed x18, local copies, waits for them, and re-layouts  2.57 us

profile of v3, /device:TPU:1, one launch (start us, length us, event | category | flops | bytes accessed | tf_op | source)
XLA Modules:
  0.0 117.7 jit_solution(12255015106437994605)
XLA Ops:
  0.0 0.0 copy-start
  0.0 0.0 copy-start.4
  0.0 0.0 copy-start.1
  0.0 0.0 copy-start.7
  0.0 0.0 copy-start.2
  0.0 0.0 copy-start.3
  0.0 0.0 copy-start.6
  0.1 0.0 copy-start.5
  0.1 1.2 %fusion = f32[384]{0:T(512)S(1)} fusion(bf16[384,512]{1,0:T(8,128)(2,1)} %param.17), kind=kLoop, calls=%fused_computation.2 | loop fusion | flops 589440 | bytes 394752 | tf_op jit(solution)/shard_map/reduce_sum | solution.py:52
  1.3 0.0 copy-done
  1.3 1.5 %fusion.6 = f32[384,384]{0,1:T(8,128)S(1)} fusion(bf16[512,384]{1,0:T(8,128)(2,1)S(1)} %copy-done, bf16[384,512]{1,0:T(8,128)(2,1)} %param.17, f32[512]{0:T(512)} %param.21, f32[384]{0:T(512)S(1)} %add_rsqrt_fusion.1), kind=kOutput, calls=%fused_computation.10 | convolution fusion | flops 151781376 | bytes 1379840 | tf_op jit(solution)/shard_map/dot_general | solution.py:703
  2.8 0.3 copy.22
  3.1 0.9 copy.26
  4.1 0.9 fusion.33
  5.1 0.8 select_convert_fusion
  5.9 0.2 fusion.22
  6.1 0.8 pad_maximum_fusion.q_ref
  6.9 0.0 copy-done.1
  6.9 0.1 fusion.3
  7.0 0.0 copy-done.7
  7.0 0.1 fusion.5
  7.2 0.0 copy-done.4
  7.2 0.1 fusion.36
  7.3 0.8 pad_maximum_fusion.1.kvm_ref
  8.1 0.0 copy-done.2
  8.1 0.0 copy-done.3
  8.2 0.7 pad_maximum_fusion.2.wkv_ref
  8.9 0.0 copy-done.6
  8.9 0.0 copy-done.5
  8.9 0.6 pad_maximum_fusion.5.gain_ref
  9.6 106.5 %whole_layer.1 = bf16[48,2048]{1,0:T(8,128)(2,1)} custom-call(bf16[2,384,256]{2,1,0:T(8,128)(2,1)} %pad_maximum_fusion.q_ref, bf16[384,384]{1,0:T(8,128)(2,1)} %pad_maximum_fusion.1.kvm_ref, bf16[64,704]{1,0:T(8,128)(2,1)} %wg_ref.1, bf16[64,704]{1,0:T(8,128)(2,1)} %wu_ref.1, bf16[64,704]{1,0:T(8,128)(2,1)} %bitcast.22, ...), custom_call_target="tpu_custom_call" | custom-call | tf_op jit(solution)/shard_map/whole_layer/pallas_call | solution.py:737
  116.1 1.6 %copy.28 = bf16[48,2048]{1,0:T(8,128)(2,1)} copy(bf16[48,2048]{1,0:T(8,128)(2,1)} %whole_layer.1) | data formatting | bytes 393216
  (12 shorter events, 0.2 us)
Async XLA Ops:
  0.0 1.3 %copy-start = (bf16[512,384]{1,0:T(8,128)(2,1)S(1)}, bf16[512,384]{1,0:T(8,128)(2,1)}, u32[]{:S(2)}) copy-start(bf16[512,384]{1,0:T(8,128)(2,1)} %param.23) | copy-start | bytes 1179652
  0.0 7.2 %copy-start.4 = (s32[384]{0:T(512)S(1)}, s32[384]{0:T(512)}, u32[]{:S(2)}) copy-start(s32[384]{0:T(512)} %param.20) | copy-start | bytes 4612
  0.0 6.9 %copy-start.1 = (bf16[384,256]{1,0:T(8,128)(2,1)S(1)}, bf16[384,256]{1,0:T(8,128)(2,1)}, u32[]{:S(2)}) copy-start(bf16[384,256]{1,0:T(8,128)(2,1)} %param.18) | copy-start | bytes 589828
  0.0 7.0 %copy-start.7 = (f32[256]{0:T(256)S(1)}, f32[256]{0:T(256)}, u32[]{:S(2)}) copy-start(f32[256]{0:T(256)} %param.22) | copy-start | bytes 3076
  0.0 8.1 %copy-start.2 = (bf16[256,256]{1,0:T(8,128)(2,1)S(1)}, bf16[256,256]{1,0:T(8,128)(2,1)}, u32[]{:S(2)}) copy-start(bf16[256,256]{1,0:T(8,128)(2,1)} %param.24) | copy-start | bytes 393220
  0.0 8.1 %copy-start.3 = (bf16[256,256]{1,0:T(8,128)(2,1)S(1)}, bf16[256,256]{1,0:T(8,128)(2,1)}, u32[]{:S(2)}) copy-start(bf16[256,256]{1,0:T(8,128)(2,1)} %param.25) | copy-start | bytes 393220
  0.0 8.9 %copy-start.6 = (f32[2048]{0:T(1024)S(1)}, f32[2048]{0:T(1024)}, u32[]{:S(2)}) copy-start(f32[2048]{0:T(1024)} %param.27) | copy-start | bytes 24580
  0.1 8.9 %copy-start.5 = (f32[2048]{0:T(1024)S(1)}, f32[2048]{0:T(1024)}, u32[]{:S(2)}) copy-start(f32[2048]{0:T(1024)} %param.31) | copy-start | bytes 24580

commit v4 on v3

--- a/solution.py
+++ b/solution.py
@@ -32,19 +32,6 @@
     frequency = rope_theta ** (-jnp.arange(0, RD, 2, dtype=jnp.float32) / RD)
     angles = positions.astype(jnp.float32)[:, None] * frequency[None, :]
     return (jnp.cos(angles), jnp.sin(angles))
-
-
-def rotate(values, cos_table, sin_table):
-    half_width = values.shape[-1] // 2
-    first_half = values[..., :half_width]
-    second_half = values[..., half_width:]
-    return jnp.concatenate(
-        [
-            first_half * cos_table - second_half * sin_table,
-            second_half * cos_table + first_half * sin_table,
-        ],
-        axis=-1,
-    )
 
 
 def rms_scaled(latent, scaling):
@@ -82,9 +69,11 @@
     def landed(self, slot, pair, index, way):
         self.copy(slot, slot, pair, index, way).wait_recv()
 
-    def finish(self):
+    def finish(self, pairs):
         for item in self.sent:
-            self.copy(*item).wait_send()
+            if any(item[2] is pair for pair in pairs):
+                self.copy(*item).wait_send()
+        self.sent = [item for item in self.sent if not any(item[2] is pair for pair in pairs)]
 
 
 class Ring:
@@ -180,120 +169,121 @@
 
 def plan(ka, kb, ga, gb, across, across2, attend, stage):
     ka.y1()
+    kb.z1()
     kb.y1(0)
-    kb.z1()
+    gb.y1(0)
     gb.z1()
-    gb.y1(0)
+    stage("query")
+    ga.y1()
     kb.zs(2)
-    kb.y1(1, 7)
+    kb.y1(7, 1)
     ka.y2()
     kb.y2(0)
-    ga.y1()
     gb.zs(2)
+    gb.y1(7)
     kb.zs(3)
-    kb.y1(2, 6)
-    kb.y2(1, 7)
+    kb.y1(6, 2)
+    kb.y2(7, 1)
     ka.z1()
     across(0, 0)
+    gb.y2(0)
     kb.y3(0)
     across(1, 0)
-    gb.y1(1)
-    kb.y2(2, 6)
+    gb.zs(3)
+    kb.zs(4)
+    kb.y1(5, 3)
+    gb.y1(2)
+    across2(0, 0)
+    kb.y2(6)
+    across2(1, 0)
+    kb.y2(2)
+    kb.y3(7)
+    across(1, 7)
     kb.y3(1)
     across(1, 1)
-    kb.y3(7)
-    across(1, 7)
-    across2(0, 0)
-    kb.zs(4)
-    kb.y1(3, 5)
-    across2(1, 0)
-    gb.zs(3)
-
-    def at_0_1():
-        across2(1, 1, 7)
-        gb.y1(2)
+    ka.zs(2)
+    across(0, 1, 7)
 
     def at_1_0():
-        ka.zs(2)
-        across(0, 1, 7)
+        gb.y3(0)
+        kb.y2(5, 3)
+        across2(1, 7)
+        ga.y2()
+        gb.y1(6)
+        across2(1, 1)
+        gb.zs(4)
+        kb.z5()
+        kb.y1(4)
+        across2(0, 1)
+
+    def at_1_1():
         kb.y3(6)
         across(1, 6)
-        kb.y2(3)
-        kb.z5()
-        kb.y1(4)
-        kb.y2(5)
         kb.y3(2)
         across(1, 2)
-        gb.y2(1)
-        across2(0, 1)
-        gb.zs(4)
-        gb.y1(5)
+        gb.y2(2)
+        kb.y3(5)
+        across(1, 5)
+        ka.zs(3)
+        across(0, 2, 6)
         kb.y3(3)
         across(1, 3)
+        across2(0, 7)
+
+    def at_2_0():
+        ga.z1()
+        gb.y1(5)
+        gb.z5()
+
+    def at_2_1():
+        across2(1, 6)
+
+    def at_3_0():
+        across2(1, 5, 2)
         kb.y2(4)
-
-    def at_1_1():
-        across2(0, 7)
-        kb.y3(5)
-        across(1, 5)
-
-    def at_2_0():
-        across2(1, 6, 2)
-        ka.zs(3)
-        across(0, 2, 6)
-        gb.y3(1)
-
-    def at_2_1():
+        gb.y2(7)
+        ka.zs(4)
+        across(0, 3, 5)
+        across2(0, 2)
+        gb.y3(2)
+        gb.y1(4)
+
+    def at_3_1():
+        across2(0, 6)
+
+    def at_4_0():
         across2(1, 3)
-        gb.z5()
-        gb.y1(4)
-
-    def at_3_0():
-        across2(1, 5)
+
+    def at_4_1():
         kb.y3(4)
         across(1, 4)
-        across2(0, 2)
-        ga.y2()
-
-    def at_3_1():
-        ka.zs(4)
-        across(0, 3, 5)
-        across2(0, 6)
         gb.y2(5)
-
-    def at_4_0():
-        across2(1, 4)
-        gb.y1(3)
-        ga.z1()
+        across2(0, 3)
 
     def at_5_0():
+        gb.y3(7)
+
+    def at_5_1():
+        across2(0, 5)
+        ga.zs(2)
+        gb.y1(1)
+
+    def at_6_0():
         ka.z5()
         across(0, 4)
-        across2(0, 3)
+        across2(1, 4)
+
+    def at_7_0():
+        gb.y2(4)
         gb.y3(5)
-        gb.y2(2)
-        across2(0, 5)
-
-    def at_5_1():
-        gb.y2(4)
-
-    def at_6_0():
+        gb.y2(6)
         across2(0, 4)
-        gb.y1(7)
-
-    def at_6_1():
-        gb.y3(2)
-
-    def at_7_0():
-        ga.zs(2)
-        gb.y3(4)
 
     def at_7_1():
-        gb.y1(6)
+        gb.y1(3)
 
     attend(
         {
-            (0, 1): at_0_1,
             (1, 0): at_1_0,
             (1, 1): at_1_1,
             (2, 0): at_2_0,
@@ -301,45 +291,60 @@
             (3, 0): at_3_0,
             (3, 1): at_3_1,
             (4, 0): at_4_0,
+            (4, 1): at_4_1,
             (5, 0): at_5_0,
             (5, 1): at_5_1,
             (6, 0): at_6_0,
-            (6, 1): at_6_1,
             (7, 0): at_7_0,
             (7, 1): at_7_1,
         }
     )
     stage("heads")
-    gb.y2(7, 0)
+    ga.zs(3)
+    gb.y3(4)
+    gb.y2(1)
+    gb.y3(6)
     stage("mix")
-    gb.y2(6)
-    ga.zs(3)
-    gb.y3(7)
     stage("norm")
     gb.y2(3)
-    gb.y3(0, 6, 3)
+    gb.y3(1)
+    ga.zs(4)
     stage("spread")
-    ga.zs(4)
+    gb.y3(3)
     stage("spread2")
     stage("gate0")
+    ga.z5()
     stage("gate1")
     stage("gate2")
-    ga.z5()
     stage("gate3")
     stage("ffn")
 
 
 def layer_kernel(
-    q_ref,
-    kvm_ref,
+    kvl_ref,
+    kvg_ref,
+    rope_ref,
+    doc_ref,
+    turn_ref,
+    qg_ref,
+    mixg_ref,
+    outg_ref,
+    ql_ref,
+    wq_ref,
+    wk_ref,
+    wv_ref,
     wg_ref,
     wu_ref,
     wd_ref,
-    wkv_ref,
     wo_ref,
     res_ref,
-    gain_ref,
     out_ref,
+    q_ref,
+    docs,
+    ql,
+    wq,
+    wk,
+    wv,
     kva,
     kvb,
     wa,
@@ -391,21 +396,21 @@
     own_rows = pl.multiple_of(c * 192 + par * 96, 32)
     res_rows = pl.multiple_of((x * 2 + c) * 48, 48)
     local = [
-        pltpu.make_async_copy(
-            kvm_ref.at[pl.ds(own_rows, A_ROWS)], kva.at[par, c, z, y], loc_sem.at[0]
-        ),
-        pltpu.make_async_copy(
-            kvm_ref.at[pl.ds(own_rows + A_ROWS, B_ROWS)], kvb.at[par, c, z, y], loc_sem.at[1]
-        ),
         pltpu.make_async_copy(wg_ref, wa.at[z, y], loc_sem.at[2]),
         pltpu.make_async_copy(wu_ref, wb.at[z, y, 0], loc_sem.at[3]),
         pltpu.make_async_copy(wd_ref, wb.at[z, y, 1], loc_sem.at[4]),
+    ]
+    query_side = [
+        pltpu.make_async_copy(ql_ref, ql, loc_sem.at[0]),
+        pltpu.make_async_copy(wq_ref, wq, loc_sem.at[1]),
+        pltpu.make_async_copy(wk_ref, wk, loc_sem.at[7]),
+        pltpu.make_async_copy(wv_ref, wv, loc_sem.at[8]),
     ]
     later = [
         pltpu.make_async_copy(wo_ref, wo, loc_sem.at[5]),
         pltpu.make_async_copy(res_ref.at[pl.ds(res_rows, 48)], res, loc_sem.at[6]),
     ]
-    for copy in local + later:
+    for copy in local + query_side + later:
         copy.start()
 
     targets = {
@@ -428,6 +433,19 @@
     m_ref[...] = jnp.full(m_ref.shape, -1e30, F32)
     l_ref[...] = jnp.zeros(l_ref.shape, F32)
     acc_ref[...] = jnp.zeros(acc_ref.shape, F32)
+
+    lane = lax.broadcasted_iota(jnp.int32, (384, 128), 1)
+    docs[...] = jnp.transpose(jnp.broadcast_to(doc_ref[...].astype(F32), (128, 384)))
+    own = pl.ds(own_rows, 96)
+    own_lane = lane[:96]
+    latent = rms_scaled(kvl_ref[own, :], kvg_ref[...])
+    rope = rope_ref[own, :].astype(F32)
+    turned = rope * turn_ref[0, own, :] + pltpu.roll(rope, 32, 1) * turn_ref[1, own, :]
+    same = docs[own, :] == (own_lane - 64).astype(F32)
+    extra = jnp.where(own_lane < 64, turned, jnp.where(same, 1.0, 0.0)).astype(BF16)
+    for keys, rows in ((kva, slice(0, A_ROWS)), (kvb, slice(A_ROWS, A_ROWS + B_ROWS))):
+        keys[par, c, z, y, :, 0:256] = latent[rows]
+        keys[par, c, z, y, :, 256:384] = extra[rows]
     for copy in local:
         copy.wait()
     pl.semaphore_wait(barrier, len(greeted))
@@ -471,24 +489,25 @@
     )
 
     keys_of = (kva, kvb)
+    core_keys, x_keys = (kp_s, kp_r), (kx_s, kx_r)
 
     def pair_with(color, d, theirs):
         own = apar if theirs else par
         slot = lambda: keys_of[color].at[own, c, zz[d]]
-        wires.start(slot, slot, (kp_s, kp_r), 16 * theirs + 8 * color + d, "c", 0)
+        wires.start(slot, slot, core_keys, 16 * theirs + 8 * color + d, "c", 0)
 
     def across(color, *steps):
         for d in steps:
             for h, way in ((0, "x+"), (1, "x-")):
                 slot = lambda d=d, h=h: keys_of[color].at[par, c, zz[d], pl.ds(2 * h, 2)]
-                wires.start(slot, slot, (kx_s, kx_r), 16 * h + 8 * color + d, way, 0)
+                wires.start(slot, slot, x_keys, 16 * h + 8 * color + d, way, 0)
             pair_with(color, d, 0)
 
     def across2(color, *steps):
         for d in steps:
             for h, way in ((0, "x+"), (1, "x-")):
                 slot = lambda: keys_of[color].at[apar, c, zz[d], pl.ds(2 * h, 2)]
-                wires.landed(slot, (kx_s, kx_r), 16 * h + 8 * color + d, way)
+                wires.landed(slot, x_keys, 16 * h + 8 * color + d, way)
             pair_with(color, d, 1)
 
     def attend_unit(u, h):
@@ -499,7 +518,7 @@
                 for color, keys in enumerate(keys_of):
                     wires.landed(
                         lambda: keys.at[own, other, at_z],
-                        (kp_s, kp_r),
+                        core_keys,
                         16 * theirs + 8 * color + d,
                         "c",
                     )
@@ -507,7 +526,9 @@
             [kva[:, :, at_z].reshape(1024, WIDE), kvb[:, :, at_z].reshape(512, WIDE)], axis=0
         )
         extra = rows[:, 256:384]
-        both = jnp.dot(rows[:, :256], wkv_ref[h], preferred_element_type=F32).astype(BF16)
+        cols_h = slice(128 * h, 128 * h + 128)
+        wkv = jnp.concatenate([wk[:, cols_h], wv[:, cols_h]], axis=1)
+        both = jnp.dot(rows[:, :256], wkv, preferred_element_type=F32).astype(BF16)
         keys = jnp.concatenate([both[:, :128], extra], axis=1)
         vals = both[:, 128:]
         s = lax.dot_general(
@@ -545,6 +566,22 @@
         wires.start(slot, slot, norm_pair, index, "c", 0)
 
     def stage(name):
+        if name == "query":
+            for copy in query_side:
+                copy.wait()
+            every = jnp.dot(
+                rms_scaled(ql[...], qg_ref[...]), wq[...], preferred_element_type=F32
+            )
+            first, mixed, last = every[:, :128], every[:, 128:256], every[:, 256:384]
+            last = pltpu.roll(last, 64, 1)
+            second = jnp.where(lane < 64, pltpu.roll(mixed, 64, 1), last)
+            same = docs[...] == (lane - 64).astype(F32)
+            apart = jnp.where(same | (lane >= 68), 0.0, -1e30)
+            for h, (plain, rotary) in enumerate(((first, mixed), (second, last))):
+                swapped = jnp.where(lane < 32, pltpu.roll(rotary, 96, 1), pltpu.roll(rotary, 32, 1))
+                turned = rotary * turn_ref[0] + swapped * turn_ref[1]
+                q_ref[h, :, 0:128] = plain.astype(BF16)
+                q_ref[h, :, 128:256] = jnp.where(lane < 64, turned, apart).astype(BF16)
         if name == "heads":
             for h in range(HEADS_DEV):
                 denom = jnp.sum(l_ref[h], axis=1, keepdims=True)
@@ -583,18 +620,22 @@
             lax.fori_loop(0, 8, mix, 0)
         if name == "norm":
             stream = resid_alpha * res[...].astype(F32) + mid[...]
-            normed[x, c] = layer_scaled(stream, gain_ref[0:1, :]).astype(BF16)
+            normed[x, c] = layer_scaled(stream, mixg_ref[...]).astype(BF16)
             own = lambda: normed.at[x, c]
-            wires.start(own, own, norm_pair, 0, "x+", 0)
-            wires.start(own, own, norm_pair, 1, "x-", 0)
+            for index, h, way in ((0, 0, "x+"), (1, 1, "x-"), (8, 1, "x+"), (9, 0, "x-")):
+                slot = lambda h=h: normed.at[x, c, :, cols(h)]
+                wires.start(slot, slot, norm_pair, index, way, 0)
             pass_on(own, 4)
         if name == "spread":
-            wires.landed(lambda: normed.at[xl, c], norm_pair, 0, "x+")
-            wires.landed(lambda: normed.at[xr, c], norm_pair, 1, "x-")
+            wires.finish((ka.pair, kb.pair, x_keys, core_keys, heads_pair))
             slot = lambda: normed.at[xl, c, :, cols(0)]
+            wires.landed(slot, norm_pair, 0, "x+")
             wires.start(slot, slot, norm_pair, 2, "x+", 0)
             slot_r = lambda: normed.at[xr, c, :, cols(1)]
+            wires.landed(slot_r, norm_pair, 1, "x-")
             wires.start(slot_r, slot_r, norm_pair, 3, "x-", 0)
+            wires.landed(lambda: normed.at[xl, c, :, cols(1)], norm_pair, 8, "x+")
+            wires.landed(lambda: normed.at[xr, c, :, cols(0)], norm_pair, 9, "x-")
             pass_on(lambda: normed.at[xl, c], 5)
             pass_on(lambda: normed.at[xr, c], 6)
         if name == "spread2":
@@ -666,16 +707,17 @@
             wires.landed(lambda: xin.at[1], x_pair, 1, "x-")
             pin[xl, :, 1024:2048] = (near_l + xin[1].astype(F32)).astype(BF16)
             x_send(5, xl, 1, "x-")
+            wires.finish((ga.pair, gb.pair, norm_pair, core_pair))
             for index, way in ((2, "x+"), (3, "x-"), (4, "x+"), (5, "x-")):
                 wires.landed(lambda: xin.at[index], x_pair, index, way)
             low = pair_sum(x, 0, 1024) + xin[4].astype(F32) + xin[3].astype(F32)
             high = pair_sum(x, 1024, 2048) + xin[2].astype(F32) + xin[5].astype(F32)
             ffn_sum = jnp.concatenate([low, high], axis=1)
             stream = resid_alpha * normed[x, c].astype(F32) + 0.5 * ffn_sum
-            out_ref[...] = layer_scaled(stream, gain_ref[1:2, :]).astype(BF16)
+            out_ref[...] = layer_scaled(stream, outg_ref[...]).astype(BF16)
 
     plan(ka, kb, ga, gb, across, across2, attend, stage)
-    wires.finish()
+    wires.finish((x_pair,))
 
 
 def body(
@@ -699,47 +741,29 @@
     tok_rows = q_latent.shape[0]
     positions = lax.axis_index(SP) * tok_rows + jnp.arange(tok_rows, dtype=jnp.int32)
     cos_table, sin_table = rope_angles(positions)
-    q_normed = rms_scaled(q_latent, q_gain)
-    queries = jnp.dot(q_normed, w_query, preferred_element_type=jnp.float32).reshape(
-        tok_rows, HEADS_DEV, NOPE + RD
-    )
-    kv_normed = rms_scaled(kv_latent, kv_gain)
-    key_rot = rotate(rope_key.astype(jnp.float32), cos_table, sin_table).astype(jnp.bfloat16)
-    slots = jnp.arange(64, dtype=jnp.int32)
-    same = doc_ids[:, None] == slots[None, :]
-    message = jnp.concatenate([kv_normed, key_rot, same.astype(BF16)], axis=1)
-    apart = jnp.where(same | (slots >= 4)[None, :], 0.0, -1e30).astype(BF16)
-    q_heads = []
-    for h in range(HEADS_DEV):
-        q_heads.append(
-            jnp.concatenate(
-                [
-                    queries[:, h, :NOPE].astype(BF16),
-                    rotate(queries[:, h, NOPE:], cos_table, sin_table).astype(BF16),
-                    apart,
-                ],
-                axis=1,
-            )
-        )
-    q_all = jnp.stack(q_heads)
-    wkv = jnp.stack(
+    turn = jnp.stack(
         [
-            jnp.concatenate([w[:, 128 * h : 128 * h + 128] for w in (w_key, w_value)], axis=1)
-            for h in range(HEADS_DEV)
+            jnp.concatenate([cos_table] * 4, axis=1),
+            jnp.concatenate([-sin_table, sin_table] * 2, axis=1),
         ]
     )
-
     any_spec = pl.BlockSpec(memory_space=pl.ANY)
     vmem_spec = pl.BlockSpec(memory_space=pltpu.VMEM)
     dma = pltpu.SemaphoreType.DMA
     vmem = pltpu.VMEM
-    sizes = (12, 40, 32, 32, 12, 40, 8, 8, 8, 6)
+    sizes = (12, 40, 32, 32, 12, 40, 8, 10, 8, 6)
     return pl.pallas_call(
         layer_kernel,
         out_shape=jax.ShapeDtypeStruct((48, 2048), BF16),
-        in_specs=[vmem_spec] + [any_spec] * 4 + [vmem_spec] + [any_spec] * 2 + [vmem_spec],
+        in_specs=[vmem_spec] * 8 + [any_spec] * 9,
         out_specs=vmem_spec,
         scratch_shapes=[
+            vmem((HEADS_DEV, tok_rows, 256), BF16),
+            vmem((tok_rows, 128), F32),
+            vmem(q_latent.shape, BF16),
+            vmem(w_query.shape, BF16),
+            vmem(w_key.shape, BF16),
+            vmem(w_value.shape, BF16),
             vmem((2, NC, NZ, NY, A_ROWS, WIDE), BF16),
             vmem((2, NC, NZ, NY, B_ROWS, WIDE), BF16),
             vmem((NZ, NY, 64, 704), BF16),
@@ -758,7 +782,7 @@
             vmem((NX, NC, 48, 2048), BF16),
             vmem((NX, 48, 2048), BF16),
             vmem((6, 48, 1024), BF16),
-            dma((8,)),
+            dma((9,)),
         ]
         + [dma((n,)) for n in sizes for _ in range(2)],
         compiler_params=pltpu.CompilerParams(
@@ -766,15 +790,23 @@
         ),
         name="whole_layer",
     )(
-        q_all,
-        message,
+        kv_latent,
+        kv_gain.reshape(1, -1),
+        jnp.concatenate([rope_key, rope_key], axis=1),
+        doc_ids.reshape(1, -1),
+        turn,
+        q_gain.reshape(1, -1),
+        mix_gain.reshape(1, -1),
+        out_gain.reshape(1, -1),
+        q_latent,
+        w_query,
+        w_key,
+        w_value,
         w_gate,
         w_up,
         w_down.T,
-        wkv,
         w_out,
         resid_stream,
-        jnp.stack([mix_gain, out_gain]),
     )
 
 

time: 118 us -> 109 us (0.924)
  Pallas kernels: 106 us -> 102 us
  other arithmetic: 6.58 us -> 2.67 us
  matrix products: 1.5 us -> 0 us
    pallas_call x1, Pallas kernels: 106 us -> 102 us  [body(): pl.pallas_call(layer_kernel, out_shape=jax.ShapeDtypeStruct((48, 2048), B...]
    another operation x7 -> x2, other arithmetic: 3.29 us -> 1.14 us  [body(): jnp.stack([jnp.concatenate([cos_table] * 4, axis=1), jnp.concatenate([-si...]
    dot_general x1 -> x0, matrix products: 1.5 us -> none  [body(): jnp.dot(q_normed, w_query, preferred_element_type=jnp.float32)]
    reduce_sum x2 -> x0, other arithmetic: 1.37 us -> none  [rms_scaled(): jnp.mean(widened * widened, axis=-1, keepdims=True) + eps_norm]
    unnamed x18 -> x2, local copies, waits for them, and re-layouts: 2.57 us -> 2.53 us
where the time goes in v4:
time: 109 us
  Pallas kernels  102 us (94%)
  local copies, waits for them, and re-layouts  3.79 us (3%)
  other arithmetic  2.67 us (2%)
    pallas_call x1, Pallas kernels, body(): pl.pallas_call(layer_kernel, out_shape=jax.ShapeDtypeStruct((48, 2048), B...  102 us
    unnamed x2, local copies, waits for them, and re-layouts  2.53 us

profile of v4, /device:TPU:1, one launch (start us, length us, event | category | flops | bytes accessed | tf_op | source)
XLA Modules:
  0.0 108.9 jit_solution(17435586594389485253)
XLA Ops:
  0.0 0.8 multiply_cosine_fusion
  0.8 0.4 maximum_bitcast_fusion
  1.2 0.8 pad_maximum_fusion.turn_ref
  1.9 0.9 copy.19
  2.9 0.7 pad_maximum_fusion.1.rope_ref
  3.6 1.3 %reshape.28.doc_ref = s32[1,384]{1,0:T(1,128)} reshape(s32[384]{0:T(512)} %param.20) | data formatting | bytes 3072 | tf_op jit(solution)/shard_map/reshape | solution.py:796
  4.9 102.5 %whole_layer.1 = bf16[48,2048]{1,0:T(8,128)(2,1)} custom-call(bf16[384,256]{1,0:T(8,128)(2,1)} %kvl_ref.1, f32[1,256]{1,0:T(1,128)} %bitcast.13, bf16[384,128]{1,0:T(8,128)(2,1)} %pad_maximum_fusion.1.rope_ref, s32[1,384]{1,0:T(1,128)} %reshape.28.doc_ref, f32[2,384,128]{2,1,0:T(8,128)} %pad_maximum_fusion.turn_ref, f32[1,512]{1,0:T(1,128)} %bitcast.12, ...), custom_call_target="tpu_custom_call" | custom-call | tf_op jit(solution)/shard_map/whole_layer/pallas_call | solution.py:755
  107.3 1.6 %copy.23 = bf16[48,2048]{1,0:T(8,128)(2,1)} copy(bf16[48,2048]{1,0:T(8,128)(2,1)} %whole_layer.1) | data formatting | bytes 393216
  (2 shorter events, 0.0 us)

commit v5 on v4

--- a/solution.py
+++ b/solution.py
@@ -29,9 +29,11 @@
 
 
 def rope_angles(positions):
-    frequency = rope_theta ** (-jnp.arange(0, RD, 2, dtype=jnp.float32) / RD)
+    lane = jnp.arange(128, dtype=jnp.int32)
+    frequency = rope_theta ** (-2.0 * (lane % 32).astype(jnp.float32) / RD)
     angles = positions.astype(jnp.float32)[:, None] * frequency[None, :]
-    return (jnp.cos(angles), jnp.sin(angles))
+    sign = jnp.where(lane % 64 < 32, -1.0, 1.0)
+    return (jnp.cos(angles), jnp.sin(angles) * sign[None, :])
 
 
 def rms_scaled(latent, scaling):
@@ -49,31 +51,27 @@
 class Wires:
     def __init__(self, targets):
         self.targets = targets
-        self.sent = []
-
-    def copy(self, src, dst, pair, index, way):
+
+    def copy(self, src, dst, pair, index, way, out=0):
         send, recv = pair
         return pltpu.make_async_remote_copy(
             src_ref=src(),
             dst_ref=dst(),
-            send_sem=send.at[index],
+            send_sem=send.at[out],
             recv_sem=recv.at[index],
             device_id=self.targets[way],
             device_id_type=MESH,
         )
 
-    def start(self, src, dst, pair, index, way, size):
-        self.copy(src, dst, pair, index, way).start()
-        self.sent.append((src, dst, pair, index, way))
+    def start(self, src, dst, pair, index, way, size, out=0):
+        self.copy(src, dst, pair, index, way, out).start()
 
     def landed(self, slot, pair, index, way):
         self.copy(slot, slot, pair, index, way).wait_recv()
 
-    def finish(self, pairs):
-        for item in self.sent:
-            if any(item[2] is pair for pair in pairs):
-                self.copy(*item).wait_send()
-        self.sent = [item for item in self.sent if not any(item[2] is pair for pair in pairs)]
+    def left(self, pair, out, as_many):
+        region = lambda: as_many
+        self.copy(region, region, pair, 0, "c", out).wait_send()
 
 
 class Ring:
@@ -85,7 +83,7 @@
         self.zz = [(self.z + d) % 8 for d in range(8)]
 
     def send(self, slot, index, way, blocks):
-        self.w.start(slot, slot, self.pair, index, way, blocks * self.block)
+        self.w.start(slot, slot, self.pair, index, way, blocks * self.block, int(way[0] == "z"))
 
     def got(self, slot, index, way="y+"):
         self.w.landed(slot, self.pair, index, way)
@@ -106,23 +104,29 @@
     def z1(self):
         self.got(lambda: self.part(self.z, self.yo, 0), 2)
         self.got(lambda: self.part(self.z, self.yo, 1), 3)
-        self.send(lambda: self.chunk(self.z, 0, 4), 4, "z+", 4)
-        self.send(lambda: self.chunk(self.z, 0, 4), 8, "z-", 4)
-
-    def zs(self, s):
+        for h in range(2):
+            self.send(lambda h=h: self.half(self.z, h), 4 + 4 * h, "z+", 2)
+            self.send(lambda h=h: self.half(self.z, h), 12 + 4 * h, "z-", 2)
+
+    def half(self, a, h):
+        return self.chunk(a, 2 * h, 2 * h + 2)
+
+    def zs(self, s, h):
         right, left = self.zz[9 - s], self.zz[s - 1]
-        self.got(lambda: self.chunk(right, 0, 4), 4 + s - 2)
-        self.got(lambda: self.chunk(left, 0, 4), 8 + s - 2)
-        if s < 4:
-            self.send(lambda: self.chunk(right, 0, 4), 4 + s - 1, "z+", 4)
-            self.send(lambda: self.chunk(left, 0, 4), 8 + s - 1, "z-", 4)
-        else:
-            self.send(lambda: self.chunk(right, 0, 2), 7, "z+", 2)
-            self.send(lambda: self.chunk(left, 2, 4), 11, "z-", 2)
+        self.got(lambda: self.half(right, h), 4 + 4 * h + s - 2)
+        self.got(lambda: self.half(left, h), 12 + 4 * h + s - 2)
+        if s < 4 or h == 0:
+            self.send(lambda: self.half(right, h), 4 + 4 * h + s - 1, "z+", 2)
+        if s < 4 or h == 1:
+            self.send(lambda: self.half(left, h), 12 + 4 * h + s - 1, "z-", 2)
 
     def z5(self):
-        self.got(lambda: self.chunk(self.zz[4], 0, 2), 7)
-        self.got(lambda: self.chunk(self.zz[4], 2, 4), 11)
+        self.got(lambda: self.half(self.zz[4], 0), 7)
+        self.got(lambda: self.half(self.zz[4], 1), 19)
+
+    def left(self, whole):
+        self.w.left(self.pair, 0, whole.at[0, pl.ds(0, 3)])
+        self.w.left(self.pair, 1, whole.at[pl.ds(0, 7)])
 
 
 class RingZY(Ring):
@@ -166,124 +170,131 @@
             self.got(lambda zz=zz: self.part(zz, self.yo, 0), 10 + 4 * d)
             self.got(lambda zz=zz: self.part(zz, self.yo, 1), 11 + 4 * d)
 
+    def left(self, whole):
+        self.w.left(self.pair, 0, whole.at[pl.ds(0, 6)])
+        self.w.left(self.pair, 1, whole.at[pl.ds(0, 7), 0])
+
 
 def plan(ka, kb, ga, gb, across, across2, attend, stage):
     ka.y1()
     kb.z1()
     kb.y1(0)
-    gb.y1(0)
     gb.z1()
     stage("query")
     ga.y1()
     kb.zs(2)
-    kb.y1(7, 1)
+    kb.y1(1, 7)
     ka.y2()
     kb.y2(0)
+    gb.y1(0)
     gb.zs(2)
-    gb.y1(7)
+    kb.y2(1)
     kb.zs(3)
     kb.y1(6, 2)
-    kb.y2(7, 1)
+    kb.y2(7)
     ka.z1()
     across(0, 0)
-    gb.y2(0)
     kb.y3(0)
     across(1, 0)
-    gb.zs(3)
-    kb.zs(4)
-    kb.y1(5, 3)
-    gb.y1(2)
+    gb.y1(7)
     across2(0, 0)
+    kb.y3(1)
+    across(1, 1)
     kb.y2(6)
     across2(1, 0)
     kb.y2(2)
+    kb.zs(4)
+    kb.y1(5)
     kb.y3(7)
     across(1, 7)
-    kb.y3(1)
-    across(1, 1)
-    ka.zs(2)
-    across(0, 1, 7)
+    kb.y1(3)
+
+    def at_0_1():
+        ka.zs(2, 0)
+        across2(1, 1)
 
     def at_1_0():
-        gb.y3(0)
-        kb.y2(5, 3)
+        ga.y2()
+        gb.zs(3)
+        gb.y2(0)
         across2(1, 7)
-        ga.y2()
-        gb.y1(6)
-        across2(1, 1)
-        gb.zs(4)
+        ka.zs(2, 1)
+        across(0, 1, 7)
         kb.z5()
         kb.y1(4)
-        across2(0, 1)
-
-    def at_1_1():
         kb.y3(6)
         across(1, 6)
         kb.y3(2)
         across(1, 2)
-        gb.y2(2)
+        kb.y2(5, 3)
+        ka.zs(3, 0)
+        gb.y1(6)
+        across2(0, 1)
+        gb.y3(0)
+        kb.y2(4)
         kb.y3(5)
         across(1, 5)
-        ka.zs(3)
-        across(0, 2, 6)
+
+    def at_1_1():
+        across2(0, 7)
         kb.y3(3)
         across(1, 3)
-        across2(0, 7)
+        gb.y1(1)
 
     def at_2_0():
-        ga.z1()
-        gb.y1(5)
-        gb.z5()
+        across2(1, 6)
+        ka.zs(3, 1)
+        across(0, 2, 6)
+        across2(1, 2)
 
     def at_2_1():
-        across2(1, 6)
+        across2(1, 5)
+        gb.zs(4)
 
     def at_3_0():
-        across2(1, 5, 2)
-        kb.y2(4)
-        gb.y2(7)
-        ka.zs(4)
-        across(0, 3, 5)
-        across2(0, 2)
-        gb.y3(2)
-        gb.y1(4)
-
-    def at_3_1():
-        across2(0, 6)
-
-    def at_4_0():
         across2(1, 3)
-
-    def at_4_1():
+        gb.y2(6)
         kb.y3(4)
         across(1, 4)
-        gb.y2(5)
+        ka.zs(4, 0)
+        ka.zs(4, 1)
+        across(0, 3)
+        across2(0, 2)
+        across(0, 5)
+        gb.y1(3)
+        ga.z1()
+
+    def at_3_1():
+        gb.z5()
+        across2(0, 6)
+
+    def at_4_0():
+        gb.y3(6)
+        across2(1, 4)
+        gb.y1(4)
+        ka.z5()
+        across(0, 4)
+
+    def at_4_1():
         across2(0, 3)
-
-    def at_5_0():
-        gb.y3(7)
 
     def at_5_1():
         across2(0, 5)
-        ga.zs(2)
-        gb.y1(1)
+        gb.y1(5)
 
     def at_6_0():
-        ka.z5()
-        across(0, 4)
-        across2(1, 4)
+        ga.zs(2, 0)
+        across2(0, 4)
 
     def at_7_0():
-        gb.y2(4)
-        gb.y3(5)
-        gb.y2(6)
-        across2(0, 4)
+        gb.y2(1)
 
     def at_7_1():
-        gb.y1(3)
+        ga.zs(2, 1)
 
     attend(
         {
+            (0, 1): at_0_1,
             (1, 0): at_1_0,
             (1, 1): at_1_1,
             (2, 0): at_2_0,
@@ -292,30 +303,37 @@
             (3, 1): at_3_1,
             (4, 0): at_4_0,
             (4, 1): at_4_1,
-            (5, 0): at_5_0,
             (5, 1): at_5_1,
             (6, 0): at_6_0,
             (7, 0): at_7_0,
             (7, 1): at_7_1,
         }
     )
+    gb.y2(4)
     stage("heads")
-    ga.zs(3)
+    gb.y2(5)
+    ga.zs(3, 0)
+    gb.y3(1)
+    gb.y2(3)
     gb.y3(4)
-    gb.y2(1)
-    gb.y3(6)
+    gb.y1(2)
     stage("mix")
+    ga.zs(3, 1)
+    gb.y3(5)
     stage("norm")
-    gb.y2(3)
-    gb.y3(1)
-    ga.zs(4)
+    ga.zs(4, 0)
+    gb.y3(3)
+    gb.y2(7)
     stage("spread")
-    gb.y3(3)
+    gb.y2(2)
+    ga.zs(4, 1)
+    gb.y3(7)
     stage("spread2")
+    gb.y3(2)
     stage("gate0")
-    ga.z5()
     stage("gate1")
     stage("gate2")
+    ga.z5()
     stage("gate3")
     stage("ffn")
 
@@ -325,7 +343,8 @@
     kvg_ref,
     rope_ref,
     doc_ref,
-    turn_ref,
+    cos_ref,
+    sin_ref,
     qg_ref,
     mixg_ref,
     outg_ref,
@@ -341,6 +360,7 @@
     out_ref,
     q_ref,
     docs,
+    ropes,
     ql,
     wq,
     wk,
@@ -435,12 +455,15 @@
     acc_ref[...] = jnp.zeros(acc_ref.shape, F32)
 
     lane = lax.broadcasted_iota(jnp.int32, (384, 128), 1)
-    docs[...] = jnp.transpose(jnp.broadcast_to(doc_ref[...].astype(F32), (128, 384)))
+    doc_row = doc_ref[...].reshape(1, 384).astype(F32)
+    docs[...] = jnp.transpose(jnp.broadcast_to(doc_row, (128, 384)))
+    rope_rows = rope_ref[...].astype(F32)
+    ropes[...] = jnp.transpose(jnp.concatenate([rope_rows, rope_rows], axis=0))
     own = pl.ds(own_rows, 96)
     own_lane = lane[:96]
     latent = rms_scaled(kvl_ref[own, :], kvg_ref[...])
-    rope = rope_ref[own, :].astype(F32)
-    turned = rope * turn_ref[0, own, :] + pltpu.roll(rope, 32, 1) * turn_ref[1, own, :]
+    rope = ropes[own, :]
+    turned = rope * cos_ref[own, :] + pltpu.roll(rope, 32, 1) * sin_ref[own, :]
     same = docs[own, :] == (own_lane - 64).astype(F32)
     extra = jnp.where(own_lane < 64, turned, jnp.where(same, 1.0, 0.0)).astype(BF16)
     for keys, rows in ((kva, slice(0, A_ROWS)), (kvb, slice(A_ROWS, A_ROWS + B_ROWS))):
@@ -494,13 +517,13 @@
     def pair_with(color, d, theirs):
         own = apar if theirs else par
         slot = lambda: keys_of[color].at[own, c, zz[d]]
-        wires.start(slot, slot, core_keys, 16 * theirs + 8 * color + d, "c", 0)
+        wires.start(slot, slot, core_keys, 16 * theirs + 8 * color + d, "c", 0, 2 * theirs + color)
 
     def across(color, *steps):
         for d in steps:
             for h, way in ((0, "x+"), (1, "x-")):
                 slot = lambda d=d, h=h: keys_of[color].at[par, c, zz[d], pl.ds(2 * h, 2)]
-                wires.start(slot, slot, x_keys, 16 * h + 8 * color + d, way, 0)
+                wires.start(slot, slot, x_keys, 16 * h + 8 * color + d, way, 0, color)
             pair_with(color, d, 0)
 
     def across2(color, *steps):
@@ -563,7 +586,7 @@
     cols = lambda h: pl.ds(1024 * h, 1024)
 
     def pass_on(slot, index):
-        wires.start(slot, slot, norm_pair, index, "c", 0)
+        wires.start(slot, slot, norm_pair, index, "c", 0, 1)
 
     def stage(name):
         if name == "query":
@@ -579,7 +602,7 @@
             apart = jnp.where(same | (lane >= 68), 0.0, -1e30)
             for h, (plain, rotary) in enumerate(((first, mixed), (second, last))):
                 swapped = jnp.where(lane < 32, pltpu.roll(rotary, 96, 1), pltpu.roll(rotary, 32, 1))
-                turned = rotary * turn_ref[0] + swapped * turn_ref[1]
+                turned = rotary * cos_ref[...] + swapped * sin_ref[...]
                 q_ref[h, :, 0:128] = plain.astype(BF16)
                 q_ref[h, :, 128:256] = jnp.where(lane < 64, turned, apart).astype(BF16)
         if name == "heads":
@@ -627,7 +650,13 @@
                 wires.start(slot, slot, norm_pair, index, way, 0)
             pass_on(own, 4)
         if name == "spread":
-            wires.finish((ka.pair, kb.pair, x_keys, core_keys, heads_pair))
+            ka.left(kva.at[par, c])
+            kb.left(kvb.at[par, c])
+            for color, keys in enumerate(keys_of):
+                wires.left(x_keys, color, keys.at[par, c])
+                wires.left(core_keys, color, keys.at[par, c])
+                wires.left(core_keys, 2 + color, keys.at[apar, c])
+            wires.left(heads_pair, 0, heads.at[pl.ds(0, 7)])
             slot = lambda: normed.at[xl, c, :, cols(0)]
             wires.landed(slot, norm_pair, 0, "x+")
             wires.start(slot, slot, norm_pair, 2, "x+", 0)
@@ -707,7 +736,11 @@
             wires.landed(lambda: xin.at[1], x_pair, 1, "x-")
             pin[xl, :, 1024:2048] = (near_l + xin[1].astype(F32)).astype(BF16)
             x_send(5, xl, 1, "x-")
-            wires.finish((ga.pair, gb.pair, norm_pair, core_pair))
+            ga.left(wa)
+            gb.left(wb)
+            wires.left(norm_pair, 0, normed.at[pl.ds(0, 3), 0])
+            wires.left(norm_pair, 1, normed.at[:, 0])
+            wires.left(core_pair, 0, pin)
             for index, way in ((2, "x+"), (3, "x-"), (4, "x+"), (5, "x-")):
                 wires.landed(lambda: xin.at[index], x_pair, index, way)
             low = pair_sum(x, 0, 1024) + xin[4].astype(F32) + xin[3].astype(F32)
@@ -717,7 +750,7 @@
             out_ref[...] = layer_scaled(stream, outg_ref[...]).astype(BF16)
 
     plan(ka, kb, ga, gb, across, across2, attend, stage)
-    wires.finish((x_pair,))
+    wires.left(x_pair, 0, xin)
 
 
 def body(
@@ -741,24 +774,19 @@
     tok_rows = q_latent.shape[0]
     positions = lax.axis_index(SP) * tok_rows + jnp.arange(tok_rows, dtype=jnp.int32)
     cos_table, sin_table = rope_angles(positions)
-    turn = jnp.stack(
-        [
-            jnp.concatenate([cos_table] * 4, axis=1),
-            jnp.concatenate([-sin_table, sin_table] * 2, axis=1),
-        ]
-    )
     any_spec = pl.BlockSpec(memory_space=pl.ANY)
     vmem_spec = pl.BlockSpec(memory_space=pltpu.VMEM)
     dma = pltpu.SemaphoreType.DMA
     vmem = pltpu.VMEM
-    sizes = (12, 40, 32, 32, 12, 40, 8, 10, 8, 6)
+    sizes = (2, 20, 2, 40, 4, 32, 2, 32, 2, 20, 2, 40, 1, 8, 2, 10, 1, 8, 1, 6)
     return pl.pallas_call(
         layer_kernel,
         out_shape=jax.ShapeDtypeStruct((48, 2048), BF16),
-        in_specs=[vmem_spec] * 8 + [any_spec] * 9,
+        in_specs=[vmem_spec] * 9 + [any_spec] * 9,
         out_specs=vmem_spec,
         scratch_shapes=[
             vmem((HEADS_DEV, tok_rows, 256), BF16),
+            vmem((tok_rows, 128), F32),
             vmem((tok_rows, 128), F32),
             vmem(q_latent.shape, BF16),
             vmem(w_query.shape, BF16),
@@ -784,7 +812,7 @@
             vmem((6, 48, 1024), BF16),
             dma((9,)),
         ]
-        + [dma((n,)) for n in sizes for _ in range(2)],
+        + [dma((n,)) for n in sizes],
         compiler_params=pltpu.CompilerParams(
             collective_id=0, has_side_effects=True, vmem_limit_bytes=60 * 1024 * 1024
         ),
@@ -792,9 +820,10 @@
     )(
         kv_latent,
         kv_gain.reshape(1, -1),
-        jnp.concatenate([rope_key, rope_key], axis=1),
-        doc_ids.reshape(1, -1),
-        turn,
+        rope_key.T,
+        doc_ids,
+        cos_table,
+        sin_table,
         q_gain.reshape(1, -1),
         mix_gain.reshape(1, -1),
         out_gain.reshape(1, -1),

time: 109 us -> 102 us (0.936)
  Pallas kernels: 102 us -> 99 us
  local copies, waits for them, and re-layouts: 3.79 us -> 1.62 us
  other arithmetic: 2.67 us -> 1.53 us
    pallas_call x1, Pallas kernels: 102 us -> 99 us  [body(): pl.pallas_call(layer_kernel, out_shape=jax.ShapeDtypeStruct((48, 2048), B...]
    mul x0 -> x1, other arithmetic: none -> 1.51 us  [rope_angles(): return (jnp.cos(angles), jnp.sin(angles) * sign[None, :])]
    reshape x1 -> x0, local copies, waits for them, and re-layouts: 1.26 us -> none  [body(): doc_ids.reshape(1, -1)]
    another operation x2 -> x0, other arithmetic: 1.14 us -> none  [body(): jnp.stack([jnp.concatenate([cos_table] * 4, axis=1), jnp.concatenate([-si...]
    unnamed x2 -> x1, local copies, waits for them, and re-layouts: 2.53 us -> 1.62 us
where the time goes in v5:
time: 102 us
  Pallas kernels  99 us (97%)
  local copies, waits for them, and re-layouts  1.62 us (2%)
  other arithmetic  1.53 us (2%)
    pallas_call x1, Pallas kernels, body(): pl.pallas_call(layer_kernel, out_shape=jax.ShapeDtypeStruct((48, 2048), B...  99 us

profile of v5, /device:TPU:1, one launch (start us, length us, event | category | flops | bytes accessed | tf_op | source)
XLA Modules:
  0.0 102.1 jit_solution(7063168692421109045)
XLA Ops:
  0.0 1.5 %fusion = (f32[384,128]{1,0:T(8,128)}, f32[384,128]{1,0:T(8,128)}) fusion(f32[128]{0:T(128)S(1)} %get-tuple-element.7, f32[128]{0:T(128)S(1)} %get-tuple-element.8, f32[384]{0:T(512)S(1)} %add_convert_fusion), kind=kLoop, calls=%fused_computation.2 | loop fusion | flops 98304 | bytes 395776 | tf_op jit(solution)/shard_map/mul | solution.py:36
  1.5 99.0 %whole_layer.1 = bf16[48,2048]{1,0:T(8,128)(2,1)} custom-call(bf16[384,256]{1,0:T(8,128)(2,1)} %kvl_ref.1, f32[1,256]{1,0:T(1,128)} %bitcast.11, bf16[64,384]{1,0:T(8,128)(2,1)} %bitcast.7, s32[384]{0:T(512)} %doc_ref.1, f32[384,128]{1,0:T(8,128)} %get-tuple-element.6.cos_ref, f32[384,128]{1,0:T(8,128)} %get-tuple-element.5.sin_ref, f32[1,512]{1,0:T(1,128)} %bitcast.10, ...), custom_call_target="tpu_custom_call" | custom-call | tf_op jit(solution)/shard_map/whole_layer/pallas_call | solution.py:782
  100.5 1.6 %copy.18 = bf16[48,2048]{1,0:T(8,128)(2,1)} copy(bf16[48,2048]{1,0:T(8,128)(2,1)} %whole_layer.1) | data formatting | bytes 393216
  (2 shorter events, 0.0 us)

commit v6 on v5

--- a/solution.py
+++ b/solution.py
@@ -176,118 +176,120 @@
 
 
 def plan(ka, kb, ga, gb, across, across2, attend, stage):
+    kb.z1()
+    gb.z1()
     ka.y1()
-    kb.z1()
     kb.y1(0)
-    gb.z1()
     stage("query")
-    ga.y1()
     kb.zs(2)
-    kb.y1(1, 7)
+    kb.y1(1)
+    kb.y2(0)
     ka.y2()
-    kb.y2(0)
+    kb.y1(7)
     gb.y1(0)
     gb.zs(2)
+    kb.zs(3)
+    kb.y1(6)
     kb.y2(1)
-    kb.zs(3)
-    kb.y1(6, 2)
-    kb.y2(7)
-    ka.z1()
-    across(0, 0)
     kb.y3(0)
     across(1, 0)
     gb.y1(7)
-    across2(0, 0)
+    kb.y1(2)
+    ka.z1()
+    across(0, 0)
     kb.y3(1)
     across(1, 1)
+    kb.y2(7)
+    across2(1, 0)
+    across2(0, 0)
     kb.y2(6)
-    across2(1, 0)
-    kb.y2(2)
     kb.zs(4)
-    kb.y1(5)
-    kb.y3(7)
-    across(1, 7)
-    kb.y1(3)
 
     def at_0_1():
+        kb.y1(3)
+        ga.y1()
         ka.zs(2, 0)
-        across2(1, 1)
 
     def at_1_0():
-        ga.y2()
-        gb.zs(3)
-        gb.y2(0)
-        across2(1, 7)
+        kb.y3(7)
+        across(1, 7)
         ka.zs(2, 1)
+        kb.y2(2)
         across(0, 1, 7)
+        kb.y1(5)
         kb.z5()
-        kb.y1(4)
+        kb.y2(3)
         kb.y3(6)
         across(1, 6)
+        gb.zs(3)
+        across2(1, 1)
+        kb.y1(4)
+        gb.y2(0)
+        ka.zs(3, 0)
+        ga.y2()
+        kb.y2(5)
+        ka.zs(3, 1)
+        across(0, 2)
+        kb.y3(3)
+        across(1, 3)
+        across2(1, 7)
+        kb.y2(4)
+        gb.y1(2)
+        across2(0, 1)
+
+    def at_1_1():
+        gb.y1(6)
         kb.y3(2)
         across(1, 2)
-        kb.y2(5, 3)
-        ka.zs(3, 0)
-        gb.y1(6)
-        across2(0, 1)
-        gb.y3(0)
-        kb.y2(4)
+        across2(0, 7)
+
+    def at_2_0():
+        across2(1, 6)
+        gb.zs(4)
+        across(0, 6)
+
+    def at_2_1():
+        across2(0, 2)
+        kb.y3(4)
+        across(1, 4)
+
+    def at_3_0():
+        across2(1, 2)
+        gb.y1(1, 3)
+        ka.zs(4, 0)
+        across2(1, 3)
         kb.y3(5)
         across(1, 5)
-
-    def at_1_1():
-        across2(0, 7)
-        kb.y3(3)
-        across(1, 3)
-        gb.y1(1)
-
-    def at_2_0():
-        across2(1, 6)
-        ka.zs(3, 1)
-        across(0, 2, 6)
-        across2(1, 2)
-
-    def at_2_1():
+        gb.y1(5)
+        ka.zs(4, 1)
+        across(0, 3, 5)
+
+    def at_3_1():
+        ga.z1()
+        across2(0, 6)
+        gb.z5()
+
+    def at_4_1():
+        across2(1, 4)
+        gb.y2(7)
         across2(1, 5)
-        gb.zs(4)
-
-    def at_3_0():
-        across2(1, 3)
-        gb.y2(6)
-        kb.y3(4)
-        across(1, 4)
-        ka.zs(4, 0)
-        ka.zs(4, 1)
-        across(0, 3)
-        across2(0, 2)
-        across(0, 5)
-        gb.y1(3)
-        ga.z1()
-
-    def at_3_1():
-        gb.z5()
-        across2(0, 6)
-
-    def at_4_0():
-        gb.y3(6)
-        across2(1, 4)
-        gb.y1(4)
+        across2(0, 3)
         ka.z5()
         across(0, 4)
 
-    def at_4_1():
-        across2(0, 3)
-
     def at_5_1():
         across2(0, 5)
-        gb.y1(5)
+        gb.y2(6)
 
     def at_6_0():
         ga.zs(2, 0)
+
+    def at_6_1():
         across2(0, 4)
+        gb.y1(4)
 
     def at_7_0():
-        gb.y2(1)
+        gb.y2(2)
 
     def at_7_1():
         ga.zs(2, 1)
@@ -301,39 +303,34 @@
             (2, 1): at_2_1,
             (3, 0): at_3_0,
             (3, 1): at_3_1,
-            (4, 0): at_4_0,
             (4, 1): at_4_1,
             (5, 1): at_5_1,
             (6, 0): at_6_0,
+            (6, 1): at_6_1,
             (7, 0): at_7_0,
             (7, 1): at_7_1,
         }
     )
-    gb.y2(4)
+    gb.y2(1)
     stage("heads")
-    gb.y2(5)
+    gb.y2(3)
     ga.zs(3, 0)
-    gb.y3(1)
-    gb.y2(3)
-    gb.y3(4)
-    gb.y1(2)
     stage("mix")
     ga.zs(3, 1)
-    gb.y3(5)
     stage("norm")
+    gb.y2(5, 4)
     ga.zs(4, 0)
-    gb.y3(3)
-    gb.y2(7)
     stage("spread")
-    gb.y2(2)
     ga.zs(4, 1)
-    gb.y3(7)
     stage("spread2")
-    gb.y3(2)
+    gb.y3(0, 7)
     stage("gate0")
+    gb.y3(6, 1)
     stage("gate1")
+    ga.z5()
+    gb.y3(3, 4)
     stage("gate2")
-    ga.z5()
+    gb.y3(5, 2)
     stage("gate3")
     stage("ffn")
 
@@ -675,7 +672,7 @@
                 wires.landed(lambda: normed.at[at, other], norm_pair, index, "c")
         if name[:4] == "gate":
             k = int(name[4:])
-            near, far = ((0, 1), (7, 2), (6, 3), (5, 4))[k]
+            near, far = ((0, 7), (6, 1), (3, 4), (5, 2))[k]
             at = [zz[near], zz[far]]
             rows = jnp.concatenate(
                 [

time: 102 us -> 100 us (0.980)
  Pallas kernels: 99 us -> 97.2 us
    pallas_call x1, Pallas kernels: 99 us -> 97.2 us  [body(): pl.pallas_call(layer_kernel, out_shape=jax.ShapeDtypeStruct((48, 2048), B...]
where the time goes in v6:
time: 100 us
  Pallas kernels  97.2 us (97%)
  local copies, waits for them, and re-layouts  1.62 us (2%)
  other arithmetic  1.53 us (2%)
    pallas_call x1, Pallas kernels, body(): pl.pallas_call(layer_kernel, out_shape=jax.ShapeDtypeStruct((48, 2048), B...  97.2 us

profile of v6, /device:TPU:1, one launch (start us, length us, event | category | flops | bytes accessed | tf_op | source)
XLA Modules:
  0.0 100.3 jit_solution(14701433623804692961)
XLA Ops:
  0.0 1.5 %fusion = (f32[384,128]{1,0:T(8,128)}, f32[384,128]{1,0:T(8,128)}) fusion(f32[128]{0:T(128)S(1)} %get-tuple-element.7, f32[128]{0:T(128)S(1)} %get-tuple-element.8, f32[384]{0:T(512)S(1)} %add_convert_fusion), kind=kLoop, calls=%fused_computation.2 | loop fusion | flops 98304 | bytes 395776 | tf_op jit(solution)/shard_map/mul | solution.py:36
  1.5 97.2 %whole_layer.1 = bf16[48,2048]{1,0:T(8,128)(2,1)} custom-call(bf16[384,256]{1,0:T(8,128)(2,1)} %kvl_ref.1, f32[1,256]{1,0:T(1,128)} %bitcast.11, bf16[64,384]{1,0:T(8,128)(2,1)} %bitcast.7, s32[384]{0:T(512)} %doc_ref.1, f32[384,128]{1,0:T(8,128)} %get-tuple-element.6.cos_ref, f32[384,128]{1,0:T(8,128)} %get-tuple-element.5.sin_ref, f32[1,512]{1,0:T(1,128)} %bitcast.10, ...), custom_call_target="tpu_custom_call" | custom-call | tf_op jit(solution)/shard_map/whole_layer/pallas_call | solution.py:779
  98.7 1.6 %copy.18 = bf16[48,2048]{1,0:T(8,128)(2,1)} copy(bf16[48,2048]{1,0:T(8,128)(2,1)} %whole_layer.1) | data formatting | bytes 393216
  (2 shorter events, 0.0 us)
